TPU v7x, 512 devices: a whole 4x4x16 slice. The times are simulated.
512 devices in a mesh: sp: 16 (over y, x), tp: 32 (over z, core).
Axes of the slice: x: 4, y: 4, z: 16, core: 2. Of those that a mesh axis runs over, the one named last changes fastest.
Arguments:
- tokens: bfloat16 [32768, 2048], P('sp', 'tp'), may hold values from -6 to 6
- norm_gain: float32 [2048], replicated, may hold values from 0.1 to 1.9
- w_key: bfloat16 [2048, 1024], P(None, 'tp'), may hold values from -0.125 to 0.125
- w_decay: bfloat16 [2048, 1024], P(None, 'tp'), may hold values from -0.125 to 0.125
- w_value: bfloat16 [2048, 512], replicated, may hold values from -0.125 to 0.125
- decay_bias: float32 [1024], P('tp'), may hold values from 0 to 8.5
- gate_drift: float32 [32768], P('sp'), may hold values from -1 to 1
- queries: bfloat16 [1024], P('tp'), may hold values from -6 to 6
- out_gain: float32 [4, 512], P(None, 'sp'), may hold values from 0.1 to 1.9
Outputs:
- state_cache: bfloat16 [1024, 512], P('tp', 'sp')
- first_read: float32 [4, 512], P(None, 'sp')
All inputs are finite; a program needn't handle non-finite values.
Results may differ from a plain program's by a relative error of at most 0.009.
Values may be sent and summed in bfloat16 or wider, within the bound.
A program may use at most 128 MiB of HBM per device.

v0:
```python
import jax
import jax.numpy as jnp
from jax import lax
from jax.sharding import PartitionSpec as P

QUERY_KEY_HEADS = 4
KEY_CHANNELS = 256
VALUE_CHANNELS = 512


EPS = 1e-06
GATE_NORM = 16.0


def copy_for_each(shard, axis):
    copies = jnp.broadcast_to(shard, (lax.axis_size(axis), *shard.shape))
    return lax.all_to_all(copies, axis, split_axis=0, concat_axis=0, tiled=True)


def taken_together(shard, axis):
    return copy_for_each(shard, axis).sum(axis=0)


def body(tokens, norm_gain, w_key, w_decay, w_value, decay_bias, gate_drift, queries, out_gain):
    gathered = lax.all_gather(tokens, "tp", axis=1, tiled=True)
    rows_f32 = gathered.astype(jnp.float32)
    inverse_rms = lax.rsqrt(jnp.mean(rows_f32 * rows_f32, axis=1, keepdims=True) + EPS)
    normed = (rows_f32 * inverse_rms * norm_gain[None, :]).astype(jnp.bfloat16)
    key_proj = jnp.dot(normed, w_key, preferred_element_type=jnp.float32).astype(jnp.bfloat16)
    gate_pre = jnp.dot(normed, w_decay, preferred_element_type=jnp.float32).astype(jnp.bfloat16)
    value_proj = jnp.dot(normed, w_value, preferred_element_type=jnp.float32).astype(jnp.bfloat16)
    log_decay = (
        jax.nn.log_sigmoid(gate_pre.astype(jnp.float32) + decay_bias[None, :] + gate_drift[:, None])
        / GATE_NORM
    )
    suffix = lax.cumsum(log_decay, axis=0, reverse=True)
    weighted = (key_proj.astype(jnp.float32) * jnp.exp(suffix - log_decay)).astype(jnp.bfloat16)
    partial_value = lax.dot_general(
        weighted, value_proj, (((0,), (0,)), ((), ())), preferred_element_type=jnp.float32
    )
    total_decay = suffix[0]
    channels = partial_value.shape[0]
    span_count = lax.axis_size("sp")
    spread = jnp.broadcast_to(total_decay[None, :, None], (1, channels, span_count))
    blocks, totals = (
        lax.all_to_all(partial_value[None], "sp", split_axis=2, concat_axis=0, tiled=True),
        lax.all_to_all(spread, "sp", split_axis=2, concat_axis=0, tiled=True),
    )
    later_sum = lax.cumsum(totals, axis=0, reverse=True) - totals
    matrix_state = jnp.sum(jnp.exp(later_sum) * blocks, axis=0)
    state_cache = matrix_state.astype(jnp.bfloat16)
    channel_ids = lax.axis_index("tp") * channels + jnp.arange(channels, dtype=jnp.int32)
    owners = (channel_ids // KEY_CHANNELS)[:, None] == jnp.arange(QUERY_KEY_HEADS, dtype=jnp.int32)[
        None, :
    ]
    query_of_head = jnp.where(
        owners, queries.astype(jnp.float32)[:, None] * KEY_CHANNELS ** (-0.5), 0.0
    )
    part_read = lax.dot_general(query_of_head, matrix_state, (((0,), (0,)), ((), ())))
    summed_read = taken_together(part_read, "tp")
    squares = taken_together(jnp.sum(summed_read * summed_read, axis=1), "sp")
    first_read = summed_read * lax.rsqrt(squares / VALUE_CHANNELS + EPS)[:, None] * out_gain
    return (state_cache, first_read)


def solution(mesh):
    return jax.shard_map(
        body,
        mesh=mesh,
        in_specs=(
            P("sp", "tp"),
            P(),
            P(None, "tp"),
            P(None, "tp"),
            P(),
            P("tp"),
            P("sp"),
            P("tp"),
            P(None, "sp"),
        ),
        out_specs=(P("tp", "sp"), P(None, "sp")),
        check_vma=False,
    )
```

profile of v0, /device:TPU:1, one launch (start us, length us, event | category | flops | bytes accessed | tf_op | source)
XLA Modules:
  0.0 233.4 jit_solution(4992811210441940215)
XLA Ops:
  7.2 0.0 copy-start
  7.2 0.0 copy-start.3
  7.2 0.0 all-gather.2.cloned.1.call-start
  7.2 0.7 all-gather.2.cloned.1.call-update
  7.9 0.7 convert_multiply_fusion.2
  8.6 86.0 %all-gather.2.cloned.1.call-done = bf16[2048,2048]{0,1:T(8,128)(2,1)} async-done(((bf16[2048,64]{0,1:T(8,128)(2,1)}), bf16[2048,2048]{0,1:T(8,128)(2,1)}) %all-gather.2.cloned.1.call-update) | async-done | bytes 8388624 | tf_op jit(solution)/shard_map/all_gather | solution.py:25
  94.6 5.1 %fusion = f32[2048]{0:T(1024)S(1)} fusion(bf16[2048,2048]{0,1:T(8,128)(2,1)} %all-gather.2.cloned.1.call-done), kind=kLoop, calls=%fused_computation.2 | loop fusion | flops 12580864 | bytes 8396800 | tf_op jit(solution)/shard_map/reduce_sum | solution.py:27
  99.7 0.0 copy-done.3
  99.7 0.0 copy-start.1
  99.8 0.0 copy-start.4
  99.8 0.0 copy-start.6
  99.8 8.6 %fusion.2 = bf16[2048,2048]{0,1:T(8,128)(2,1)} fusion(bf16[2048,2048]{0,1:T(8,128)(2,1)} %all-gather.2.cloned.1.call-done, f32[2048]{0:T(1024)S(1)} %copy-done.3, f32[2048]{0:T(1024)S(1)} %add_rsqrt_fusion), kind=kLoop, calls=%fused_computation.4 | loop fusion | flops 16777216 | bytes 16793600 | tf_op jit(solution)/shard_map/convert_element_type | solution.py:28
  108.4 0.0 copy-done.1
  108.4 0.0 copy-done.4
  108.4 0.0 copy-done.6
  108.4 0.0 copy-start.2
  108.4 5.0 %fusion.9 = f32[2048,32]{0,1:T(8,128)S(1)} fusion(bf16[2048,32]{0,1:T(8,128)(2,1)S(1)} %copy-done.1, bf16[2048,2048]{0,1:T(8,128)(2,1)} %fusion.2, f32[2048]{0:T(1024)S(1)} %copy-done.4, f32[32]{0:T(128)S(1)} %copy-done.6), kind=kOutput, calls=%fused_computation.14 | convolution fusion | flops 268763136 | bytes 8790144 | tf_op jit(solution)/shard_map/dot_general | solution.py:30
  113.4 0.2 fusion.13
  113.6 39.7 %reduce-window.6 = f32[32,16,128]{2,1,0:T(8,128)S(1)} reduce-window(f32[32,16,128]{2,1,0:T(8,128)S(1)} %bitcast.59, f32[]{:T(128)} %constant.32.clone.1), window={size=1x1x128 pad=0_0x0_0x0_127}, to_apply=%region_1.2 | reduce-window | flops 8323072 | bytes 524292 | tf_op jit(solution)/shard_map/reduce-window
  153.3 0.2 copy.32
  153.5 0.2 reduce-window.9
  153.7 0.1 slice.13
  153.8 0.1 broadcast_add_fusion
  153.9 0.1 copy.40
  154.0 0.0 copy-done.2
  154.0 5.0 %fusion.5 = bf16[2048,32]{0,1:T(8,128)(2,1)S(1)} fusion(bf16[2048,32]{0,1:T(8,128)(2,1)S(1)} %copy-done.2, bf16[2048,2048]{0,1:T(8,128)(2,1)} %fusion.2, f32[2048,32]{0,1:T(8,128)S(1)} %fusion.9, f32[4,8,16,128]{3,2,1,0:T(8,128)S(1)} %bitcast.56), kind=kOutput, calls=%fused_computation.9 | convolution fusion | flops 269287424 | bytes 9175040 | tf_op jit(solution)/shard_map/dot_general | solution.py:29
  159.0 0.1 slice_reduce_fusion
  159.2 0.6 broadcast_in_dim.37
  159.8 6.6 %all-to-all-start = ((f32[1,32,16]{1,0,2:T(1,128)}), f32[1,32,16]{1,0,2:T(1,128)S(1)}, u32[]{:S(2)}, u32[]{:S(2)}) async-start(f32[1,32,16]{1,0,2:T(1,128)} %broadcast_in_dim.37), calls=%async_computation | async-start | bytes 16384 | tf_op jit(solution)/shard_map/all_to_all | solution.py:47
  166.4 0.0 copy-done
  166.4 0.0 copy-start.5
  166.4 9.2 %fusion.10 = f32[32,512]{0,1:T(8,128)S(1)} fusion(bf16[2048,32]{0,1:T(8,128)(2,1)S(1)} %fusion.5, bf16[2048,2048]{0,1:T(8,128)(2,1)} %fusion.2, bf16[2048,512]{1,0:T(8,128)(2,1)S(1)} %copy-done), kind=kOutput, calls=%fused_computation.15 | convolution fusion | flops 4363124736 | bytes 10682368 | tf_op jit(solution)/shard_map/dot_general | solution.py:38
  175.7 0.5 broadcast.91
  176.2 1.3 reduce.3
  177.5 0.8 reshape.75
  178.3 0.0 all-to-all-done
  178.3 6.6 %all-to-all-start.1 = ((f32[16,1,1024]{2,1,0:T(1,128)}), f32[16,1,1024]{2,1,0:T(1,128)S(1)}, u32[]{:S(2)}, u32[]{:S(2)}) async-start(f32[16,1,1024]{2,1,0:T(1,128)} %reshape.75), calls=%async_computation.1 | async-start | bytes 131072 | tf_op jit(solution)/shard_map/all_to_all | solution.py:46
  185.0 6.5 %all-to-all-done.1 = f32[16,1,1024]{2,1,0:T(1,128)S(1)} async-done(((f32[16,1,1024]{2,1,0:T(1,128)}), f32[16,1,1024]{2,1,0:T(1,128)S(1)}, u32[]{:S(2)}, u32[]{:S(2)}) %all-to-all-start.1) | async-done | bytes 65568 | tf_op jit(solution)/shard_map/all_to_all | solution.py:46
  191.4 0.8 reduce.4
  192.2 0.4 reshape.76
  192.7 0.2 fusion.22
  193.0 0.1 reshape.77
  193.1 21.4 %all_to_all.44 = f32[32,1,128]{2,1,0:T(1,128)S(1)} all-to-all(f32[32,1,128]{2,1,0:T(1,128)S(1)} %reshape.77), channel_id=1, replica_groups=mesh['sp'=16,'tp'=32] {'tp'}, dimensions={0} | all-to-all | bytes 32768 | tf_op jit(solution)/shard_map/all_to_all | solution.py:17
  214.5 0.7 reduce.5
  215.2 0.1 reshape.78
  215.3 0.1 multiply_reduce_fusion.1
  215.4 0.6 broadcast_in_dim.42
  216.0 3.5 %all-to-all-start.3 = ((f32[16,1,4]{2,1,0:T(1,128)}), f32[16,1,4]{2,1,0:T(1,128)S(1)}, u32[]{:S(2)}, u32[]{:S(2)}) async-start(f32[16,1,4]{2,1,0:T(1,128)} %broadcast_in_dim.42), calls=%async_computation.3 | async-start | bytes 16384 | tf_op jit(solution)/shard_map/all_to_all | solution.py:17
  219.5 0.7 copy.31
  220.2 5.7 %all-to-all-done.3 = f32[16,1,4]{2,1,0:T(1,128)S(1)} async-done(((f32[16,1,4]{2,1,0:T(1,128)}), f32[16,1,4]{2,1,0:T(1,128)S(1)}, u32[]{:S(2)}, u32[]{:S(2)}) %all-to-all-start.3) | async-done | bytes 288 | tf_op jit(solution)/shard_map/all_to_all | solution.py:17
  225.9 0.0 copy-done.5
  225.9 0.7 multiply_multiply_fusion
  (10 shorter events, 0.3 us)
Async XLA Ops:
  7.2 159.2 %copy-start = (bf16[2048,512]{1,0:T(8,128)(2,1)S(1)}, bf16[2048,512]{1,0:T(8,128)(2,1)}, u32[]{:S(2)}) copy-start(bf16[2048,512]{1,0:T(8,128)(2,1)} %param.13) | copy-start | bytes 6291460
  7.2 92.6 %copy-start.3 = (f32[2048]{0:T(1024)S(1)}, f32[2048]{0:T(1024)}, u32[]{:S(2)}) copy-start(f32[2048]{0:T(1024)} %param.10) | copy-start | bytes 24580
  7.2 87.4 %all-gather.2.cloned.1.call-start = ((), (), s32[]{:S(2)}) async-start(), calls=%async_computation.4 | async-start | bytes 8650752 | tf_op jit(solution)/shard_map/all_gather | solution.py:25
  99.7 8.6 %copy-start.1 = (bf16[2048,32]{0,1:T(8,128)(2,1)S(1)}, bf16[2048,32]{0,1:T(8,128)(2,1)}, u32[]{:S(2)}) copy-start(bf16[2048,32]{0,1:T(8,128)(2,1)} %param.12) | copy-start | bytes 393220
  99.8 8.6 %copy-start.4 = (f32[2048]{0:T(1024)S(1)}, f32[2048]{0:T(1024)}, u32[]{:S(2)}) copy-start(f32[2048]{0:T(1024)} %param.15) | copy-start | bytes 24580
  99.8 8.6 %copy-start.6 = (f32[32]{0:T(128)S(1)}, f32[32]{0:T(128)}, u32[]{:S(2)}) copy-start(f32[32]{0:T(128)} %param.14) | copy-start | bytes 388
  108.4 45.6 %copy-start.2 = (bf16[2048,32]{0,1:T(8,128)(2,1)S(1)}, bf16[2048,32]{0,1:T(8,128)(2,1)}, u32[]{:S(2)}) copy-start(bf16[2048,32]{0,1:T(8,128)(2,1)} %param.11) | copy-start | bytes 393220
  159.8 18.5 %all-to-all-start = ((f32[1,32,16]{1,0,2:T(1,128)}), f32[1,32,16]{1,0,2:T(1,128)S(1)}, u32[]{:S(2)}, u32[]{:S(2)}) async-start(f32[1,32,16]{1,0,2:T(1,128)} %broadcast_in_dim.37), calls=%async_computation | async-start | bytes 16384 | tf_op jit(solution)/shard_map/all_to_all | solution.py:47
  166.4 59.5 %copy-start.5 = (f32[4,32]{1,0:T(4,128)S(1)}, f32[4,32]{1,0:T(4,128)}, u32[]{:S(2)}) copy-start(f32[4,32]{1,0:T(4,128)} %param.17) | copy-start | bytes 1540
  178.3 13.2 %all-to-all-start.1 = ((f32[16,1,1024]{2,1,0:T(1,128)}), f32[16,1,1024]{2,1,0:T(1,128)S(1)}, u32[]{:S(2)}, u32[]{:S(2)}) async-start(f32[16,1,1024]{2,1,0:T(1,128)} %reshape.75), calls=%async_computation.1 | async-start | bytes 131072 | tf_op jit(solution)/shard_map/all_to_all | solution.py:46
  216.0 9.9 %all-to-all-start.3 = ((f32[16,1,4]{2,1,0:T(1,128)}), f32[16,1,4]{2,1,0:T(1,128)S(1)}, u32[]{:S(2)}, u32[]{:S(2)}) async-start(f32[16,1,4]{2,1,0:T(1,128)} %broadcast_in_dim.42), calls=%async_computation.3 | async-start | bytes 16384 | tf_op jit(solution)/shard_map/all_to_all | solution.py:17
Sparse Core Ops, SparseCore 0:
  10.1 84.4 all-gather.1
where the time goes:
time: 234 us; the launch traced here: 233 us
  waiting for transfers between devices  98.8 us (42%)
  other arithmetic  58.3 us (25%)
  blocking collectives  21.4 us (9%)
  matrix products  19.5 us (8%)
  starting transfers between devices  16.8 us (7%)
  between operations  14.3 us (6%)
  local copies, waits for them, and re-layouts  4.45 us (2%)
    all_gather x1, waiting for transfers between devices, body(): gathered = lax.all_gather(tokens, 'tp', axis=1, tiled=True)  86 us
    another operation x2, other arithmetic  39.9 us
    all_to_all x1, blocking collectives, copy_for_each(): return lax.all_to_all(copies, axis, split_axis=0, concat_axis=0, tiled=True)  21.4 us
    dot_general x1, matrix products, body(): lax.dot_general(weighted, value_proj, (((0,), (0,)), ((), ())), preferred...  9.21 us
    convert_element_type x1, other arithmetic, body(): normed = (rows_f32 * inverse_rms * norm_gain[None, :]).astype(jnp.bfloat16)  8.58 us
    all_to_all x1, starting transfers between devices, body(): lax.all_to_all(partial_value[None], 'sp', split_axis=2, concat_axis=0, ti...  6.65 us
    all_to_all x1, starting transfers between devices, body(): lax.all_to_all(spread, 'sp', split_axis=2, concat_axis=0, tiled=True)  6.63 us
    all_to_all x1, waiting for transfers between devices, body(): lax.all_to_all(partial_value[None], 'sp', split_axis=2, concat_axis=0, ti...  6.47 us
  transfers between devices with their start and end apart: 4, of which 3 were waited for; matrix products, arithmetic and copies ran while one was open for 6% of the time, Pallas kernels for 0%

commit v1 on v0

v1 whole, which is shorter than its diff:
```python
import functools

import jax
import jax.numpy as jnp
from jax import lax
from jax.experimental import pallas as pl
from jax.experimental.pallas import tpu as pltpu
from jax.sharding import PartitionSpec as P

MESH = pl.DeviceIdType.MESH
EPS = 1e-06
GATE_NORM = 16.0
KEY_CHANNELS = 256
N_SP, N_TP, N_Z = 16, 32, 16
SPAN, FEATS, VALS, CH = 2048, 64, 512, 32
HALF = SPAN // 2
VT = 32
HEADS = 4
MODEL = N_TP * FEATS
TILE = 512


def column_of(row):
    n = row.shape[1]
    on_diagonal = lax.broadcasted_iota(jnp.int32, (n, n), 0) == lax.broadcasted_iota(jnp.int32, (n, n), 1)
    return jnp.sum(jnp.where(on_diagonal, jnp.broadcast_to(row, (n, n)), 0.0), axis=1, keepdims=True)


def tile_of(col, group):
    out = jnp.broadcast_to(col[0:8], (8, 128))
    for a in range(1, 4):
        out = jnp.where(group == a, jnp.broadcast_to(col[8 * a : 8 * a + 8], (8, 128)), out)
    return out


def kernel(
    x_ref, gain_ref, wk_ref, wd_ref, wv_ref, bias_ref, drift_ref, q_ref, og_ref,
    state_ref, read_ref,
    xt, wt, acc, squares, vt_bf, msg, got, read_msg, read_got, sq_msg, sq_got,
    ring_send, ring_recv, pair_send, pair_recv,
    p_send, p_recv, r_send, r_recv, s_send, s_recv,
):
    j = lax.axis_index("sp")
    t = lax.axis_index("tp")
    z, k = t // 2, t % 2
    sibling = 2 * z + 1 - k
    up = 2 * lax.rem(z + 1, N_Z) + k
    down = 2 * lax.rem(z + N_Z - 1, N_Z) + k

    barrier = pltpu.get_barrier_semaphore()
    for other in (sibling, up, down):
        pl.semaphore_signal(barrier, inc=1, device_id=(j, other), device_id_type=MESH)

    @pl.loop(1, N_SP)
    def _(o):
        pl.semaphore_signal(barrier, inc=1, device_id=(lax.rem(j + o, N_SP), t), device_id_type=MESH)

    pl.semaphore_wait(barrier, 3 + N_SP - 1)

    def rows_of(src_z, core):
        return pl.ds(pl.multiple_of((2 * src_z + core) * FEATS, FEATS), FEATS)

    def lanes_of(sub):
        return pl.ds(sub * HALF, HALF)

    def ring(way, sub, s):
        src_z = lax.rem(z - (s - 1) + 2 * N_Z, N_Z) if way == 0 else lax.rem(z + (s - 1), N_Z)
        place = xt.at[rows_of(src_z, k), lanes_of(sub)]
        if isinstance(s, int) and s == 1:
            source = x_ref.at[:, lanes_of(sub)]
        else:
            source = place
        return pltpu.make_async_remote_copy(
            src_ref=source, dst_ref=place,
            send_sem=ring_send.at[way, sub, s], recv_sem=ring_recv.at[way, sub, s],
            device_id=(j, up if way == 0 else down), device_id_type=MESH,
        )

    def pair(src_z, sub, slot, own=False):
        place = xt.at[rows_of(src_z, k), lanes_of(sub)]
        return pltpu.make_async_remote_copy(
            src_ref=x_ref.at[:, lanes_of(sub)] if own else place, dst_ref=place,
            send_sem=pair_send.at[slot, sub], recv_sem=pair_recv.at[slot, sub],
            device_id=(j, sibling), device_id_type=MESH,
        )

    for sub in range(2):
        for way in range(2):
            ring(way, sub, 1).start()
    for sub in range(2):
        pair(z, sub, 0, own=True).start()

    xt[rows_of(z, k), :] = x_ref[...]
    gain = gain_ref[...]
    wt[0:CH, :] = (wk_ref[...].astype(jnp.float32) * gain).astype(jnp.bfloat16)
    wt[CH : 2 * CH, :] = (wd_ref[...].astype(jnp.float32) * gain).astype(jnp.bfloat16)

    def weights(src_z):
        feats = pl.ds(pl.multiple_of(src_z * 2 * FEATS, 2 * FEATS), 2 * FEATS)
        wv_t = wv_ref[feats, :].astype(jnp.float32).T * gain_ref[:, feats]
        return jnp.concatenate([wv_t.astype(jnp.bfloat16), wt[:, feats]], axis=0)

    def compute(sub, sources, first):
        ws = [weights(src) for src in sources]

        @pl.loop(0, HALF // TILE)
        def _(i):
            lanes = pl.ds(pl.multiple_of(sub * HALF + i * TILE, TILE), TILE)
            total = None
            sq = None
            for src, w in zip(sources, ws):
                x = xt[pl.ds(pl.multiple_of(src * 2 * FEATS, 2 * FEATS), 2 * FEATS), lanes]
                term = jnp.dot(w, x, preferred_element_type=jnp.float32)
                total = term if total is None else total + term
                xf = x.astype(jnp.float32)
                part = jnp.sum((xf * xf).reshape(2 * FEATS // 8, 8, TILE), axis=0)
                sq = part if sq is None else sq + part
            if first:
                acc[:, lanes] = total
                squares[:, lanes] = sq
            else:
                acc[:, lanes] += total
                squares[:, lanes] += sq

    for sub in range(2):
        pair(z, sub, 0).wait_recv()
        compute(sub, [z], True)

    def above(s):
        return lax.rem(z + s, N_Z)

    def below(s):
        return lax.rem(z - s + 2 * N_Z, N_Z)

    @pl.loop(1, 8)
    def _(s):
        for sub in range(2):
            ring(0, sub, s).wait_recv()
            if sub == 0:
                ring(0, sub, s + 1).start()
            else:
                @pl.when(s < 7)
                def _():
                    ring(0, sub, s + 1).start()
            pair(below(s), sub, s).start()
            ring(1, sub, s).wait_recv()
            if sub == 1:
                ring(1, sub, s + 1).start()
            else:
                @pl.when(s < 7)
                def _():
                    ring(1, sub, s + 1).start()
            pair(above(s), sub, 8 + s).start()

            @pl.when(s > 1)
            def _():
                pair(below(s - 1), sub, s - 1).wait_recv()
                pair(above(s - 1), sub, 7 + s).wait_recv()
                compute(sub, [below(s - 1), above(s - 1)], False)

    for sub in range(2):
        ring(sub, sub, 8).wait_recv()
        pair(below(8), sub, 8).start()
        pair(below(7), sub, 7).wait_recv()
        pair(above(7), sub, 15).wait_recv()
        compute(sub, [below(7), above(7)], False)
    for sub in range(2):
        pair(below(8), sub, 8).wait_recv()
        compute(sub, [below(8)], False)

    inverse = lax.rsqrt(jnp.sum(squares[...], axis=0, keepdims=True) * (1.0 / MODEL) + EPS)
    key = (acc[VALS : VALS + CH, :] * inverse).astype(jnp.bfloat16).astype(jnp.float32)
    gate = (acc[VALS + CH : VALS + 2 * CH, :] * inverse).astype(jnp.bfloat16).astype(jnp.float32)

    @pl.loop(0, VALS // 64)
    def _(i):
        rows = pl.ds(pl.multiple_of(i * 64, 64), 64)
        vt_bf[rows, :] = (acc[rows, :] * inverse).astype(jnp.bfloat16)

    u = gate + column_of(bias_ref[...]) + drift_ref[...]
    log_decay = (jnp.minimum(u, 0.0) - jnp.log1p(jnp.exp(-jnp.abs(u)))) * (1.0 / GATE_NORM)
    blocks = SPAN // 128
    stacked = jnp.concatenate([log_decay[:, 128 * b : 128 * b + 128] for b in range(blocks)], axis=0)
    after = lax.broadcasted_iota(jnp.int32, (128, 128), 0) > lax.broadcasted_iota(jnp.int32, (128, 128), 1)
    local = jnp.dot(
        stacked, jnp.where(after, 1.0, 0.0), precision=lax.Precision.HIGHEST,
        preferred_element_type=jnp.float32,
    )
    sums = jnp.sum(stacked, axis=1, keepdims=True)
    run = jnp.zeros((CH, 1), jnp.float32)
    pieces = [None] * blocks
    for b in reversed(range(blocks)):
        rest = local[CH * b : CH * b + CH] + run
        pieces[b] = (key[:, 128 * b : 128 * b + 128] * jnp.exp(rest)).astype(jnp.bfloat16)
        run = run + sums[CH * b : CH * b + CH]
    weighted = jnp.concatenate(pieces, axis=1)
    partial = lax.dot_general(
        weighted, vt_bf[...], (((1,), (1,)), ((), ())), preferred_element_type=jnp.float32
    )

    group = lax.broadcasted_iota(jnp.int32, (8, 128), 1) // VT
    decay_tile = tile_of(run, group)
    for c in range(4):
        quarter = [partial[8 * a : 8 * a + 8, 128 * c : 128 * c + 128] for a in range(4)]
        for d in range(4):
            out = None
            for a in range(4):
                shift = (VT * (a - d)) % 128
                moved = quarter[a] if shift == 0 else pltpu.roll(quarter[a], shift, 1)
                out = moved if out is None else jnp.where(group == a, moved, out)
            msg[4 * c + d, 0:8, :] = out
            msg[4 * c + d, 8:16, :] = decay_tile

    def exchange(o):
        to = lax.rem(j + o, N_SP)
        return pltpu.make_async_remote_copy(
            src_ref=msg.at[to], dst_ref=got.at[j], send_sem=p_send.at[o], recv_sem=p_recv.at[o],
            device_id=(to, t), device_id_type=MESH,
        )

    @pl.loop(1, N_SP)
    def _(o):
        exchange(o).start()

    got[j] = msg[j]
    q_tile = tile_of(column_of(q_ref[...].astype(jnp.float32)) * KEY_CHANNELS ** (-0.5), group)

    @pl.loop(1, N_SP)
    def _(o):
        exchange(o).wait_recv()

    later = jnp.zeros((8, 128), jnp.float32)
    state = jnp.zeros((8, 128), jnp.float32)
    for i in reversed(range(N_SP)):
        state = state + jnp.exp(later) * got[i, 0:8, :]
        later = later + got[i, 8:16, :]
    read_msg[...] = jnp.sum(q_tile * state, axis=0, keepdims=True)

    def tell(o):
        return pltpu.make_async_remote_copy(
            src_ref=read_msg, dst_ref=read_got.at[t], send_sem=r_send.at[o], recv_sem=r_recv.at[o],
            device_id=(j, lax.rem(t + o, N_TP)), device_id_type=MESH,
        )

    @pl.loop(1, N_TP)
    def _(o):
        tell(o).start()

    read_got[t] = read_msg[...]
    state_ref[...] = jnp.concatenate([state[:, VT * a : VT * a + VT] for a in range(4)], axis=0).astype(jnp.bfloat16)

    @pl.loop(1, N_TP)
    def _(o):
        tell(o).wait_recv()

    lane_group = lax.broadcasted_iota(jnp.int32, (1, 128), 1) // VT
    reads = []
    sq = jnp.zeros((1, 128), jnp.float32)
    for h in range(HEADS):
        total = read_got[8 * h]
        for i in range(1, 8):
            total = total + read_got[8 * h + i]
        total = total + pltpu.roll(total, 64, 1)
        total = total + pltpu.roll(total, 32, 1)
        reads.append(total)
        own = jnp.sum(jnp.where(lane_group == 0, total * total, 0.0), axis=1, keepdims=True)
        sq = jnp.where(lane_group == h, jnp.broadcast_to(own, (1, 128)), sq)
    sq_msg[...] = sq

    def share(o):
        return pltpu.make_async_remote_copy(
            src_ref=sq_msg, dst_ref=sq_got.at[j], send_sem=s_send.at[o], recv_sem=s_recv.at[o],
            device_id=(lax.rem(j + o, N_SP), t), device_id_type=MESH,
        )

    @pl.loop(1, N_SP)
    def _(o):
        share(o).start()

    sq_got[j] = sq_msg[...]

    @pl.loop(1, N_SP)
    def _(o):
        share(o).wait_recv()

    whole = sq_got[0]
    for i in range(1, N_SP):
        whole = whole + sq_got[i]
    scale = lax.rsqrt(whole * (1.0 / VALS) + EPS)
    for h in range(HEADS):
        factor = scale[:, VT * h : VT * h + VT]
        read_ref[h : h + 1, :] = reads[h][:, 0:VT] * factor * og_ref[h : h + 1, :]

    @pl.loop(1, 8)
    def _(s):
        for sub in range(2):
            for way in range(2):
                ring(way, sub, s).wait_send()
            pair(below(s), sub, s).wait_send()
            pair(above(s), sub, 8 + s).wait_send()

    for sub in range(2):
        ring(sub, sub, 8).wait_send()
        pair(z, sub, 0).wait_send()
        pair(below(8), sub, 8).wait_send()

    @pl.loop(1, N_SP)
    def _(o):
        exchange(o).wait_send()
        share(o).wait_send()

    @pl.loop(1, N_TP)
    def _(o):
        tell(o).wait_send()


def body(tokens, norm_gain, w_key, w_decay, w_value, decay_bias, gate_drift, queries, out_gain):
    dma = pltpu.SemaphoreType.DMA
    vmem = pl.BlockSpec(memory_space=pltpu.VMEM)
    f32, bf16 = jnp.float32, jnp.bfloat16
    return pl.pallas_call(
        kernel,
        out_shape=(jax.ShapeDtypeStruct((CH, VT), bf16), jax.ShapeDtypeStruct((HEADS, VT), f32)),
        in_specs=[vmem] * 9,
        out_specs=(vmem, vmem),
        scratch_shapes=[
            pltpu.VMEM((MODEL, SPAN), bf16),
            pltpu.VMEM((2 * CH, MODEL), bf16),
            pltpu.VMEM((VALS + 2 * CH, SPAN), f32),
            pltpu.VMEM((8, SPAN), f32),
            pltpu.VMEM((VALS, SPAN), bf16),
            pltpu.VMEM((N_SP, 16, 128), f32),
            pltpu.VMEM((N_SP, 16, 128), f32),
            pltpu.VMEM((1, 128), f32),
            pltpu.VMEM((N_TP, 1, 128), f32),
            pltpu.VMEM((1, 128), f32),
            pltpu.VMEM((N_SP, 1, 128), f32),
            dma((2, 2, 9)), dma((2, 2, 9)), dma((16, 2)), dma((16, 2)),
            dma((N_SP,)), dma((N_SP,)), dma((N_TP,)), dma((N_TP,)), dma((N_SP,)), dma((N_SP,)),
        ],
        compiler_params=pltpu.CompilerParams(
            collective_id=0, has_side_effects=True, vmem_limit_bytes=50 * 1024 * 1024
        ),
    )(
        tokens.T, norm_gain.reshape(1, MODEL), w_key.T, w_decay.T, w_value, decay_bias.reshape(1, CH),
        gate_drift.reshape(1, SPAN), queries.reshape(1, CH), out_gain,
    )


def solution(mesh):
    return jax.shard_map(
        body,
        mesh=mesh,
        in_specs=(
            P("sp", "tp"), P(), P(None, "tp"), P(None, "tp"), P(), P("tp"), P("sp"), P("tp"), P(None, "sp"),
        ),
        out_specs=(P("tp", "sp"), P(None, "sp")),
        check_vma=False,
    )
```

time: 234 us -> 94.7 us (0.40)
  waiting for transfers between devices: 98.8 us -> 0 us
  Pallas kernels: 0 us -> 84.7 us
  other arithmetic: 58.3 us -> 0 us
  blocking collectives: 21.4 us -> 0 us
  matrix products: 19.5 us -> 0 us
  starting transfers between devices: 16.8 us -> 0 us
  between operations: 14.3 us -> 0.66 us
  local copies, waits for them, and re-layouts: 4.45 us -> 8.9 us
    all_gather x1 -> x0, waiting for transfers between devices: 86 us -> none  [body(): gathered = lax.all_gather(tokens, 'tp', axis=1, tiled=True)]
    pallas_call x0 -> x1, Pallas kernels: none -> 84.7 us  [body(): pl.pallas_call(kernel, out_shape=(jax.ShapeDtypeStruct((CH, VT), bf16), j...]
    another operation x4 -> x0, other arithmetic: 40.1 us -> none
    all_to_all x1 -> x0, blocking collectives: 21.4 us -> none  [copy_for_each(): return lax.all_to_all(copies, axis, split_axis=0, concat_axis=0, tiled=True)]
    dot_general x4 -> x0, matrix products: 19.5 us -> none  [the longest x1 9.21 us: body(): lax.dot_general(weighted, value_proj, (((0,), (0,)), ((), ())), preferred...]
    all_to_all x3 -> x0, starting transfers between devices: 16.8 us -> none  [the longest x1 6.65 us: body(): lax.all_to_all(partial_value[None], 'sp', split_axis=2, concat_axis=0, ti...]
    all_to_all x3 -> x0, waiting for transfers between devices: 12.2 us -> none  [the longest x1 6.47 us: body(): lax.all_to_all(partial_value[None], 'sp', split_axis=2, concat_axis=0, ti...]
    convert_element_type x1 -> x0, other arithmetic: 8.58 us -> none  [body(): normed = (rows_f32 * inverse_rms * norm_gain[None, :]).astype(jnp.bfloat16)]
  transfers between devices with their start and end apart: 4 -> 0, of which waited for: 3 -> 0; matrix products, arithmetic and copies ran while one was open for 6% -> 0% of each run, Pallas kernels for 0% -> 0%
where the time goes in v1:
time: 94.7 us; the launch traced here: 94.3 us
  Pallas kernels  84.7 us (89%)
  local copies, waits for them, and re-layouts  8.9 us (9%)
    pallas_call x1, Pallas kernels, body(): pl.pallas_call(kernel, out_shape=(jax.ShapeDtypeStruct((CH, VT), bf16), j...  84.7 us
    unnamed x20, local copies, waits for them, and re-layouts  8.9 us

profile of v1, /device:TPU:1, one launch (start us, length us, event | category | flops | bytes accessed | tf_op | source)
XLA Modules:
  0.0 94.3 jit_solution(6958827091311373681)
XLA Ops:
  0.6 0.0 copy-start
  0.6 1.6 %copy-done = bf16[2048,512]{1,0:T(8,128)(2,1)S(1)} copy-done((bf16[2048,512]{1,0:T(8,128)(2,1)S(1)}, bf16[2048,512]{1,0:T(8,128)(2,1)}, u32[]{:S(2)}) %copy-start) | copy-done | bytes 2097176
  2.2 0.0 copy-start.1
  2.2 0.9 %copy-done.1 = bf16[2048,64]{0,1:T(8,128)(2,1)S(1)} copy-done((bf16[2048,64]{0,1:T(8,128)(2,1)S(1)}, bf16[2048,64]{0,1:T(8,128)(2,1)}, u32[]{:S(2)}) %copy-start.1) | copy-done | bytes 262168
  3.2 0.0 copy-start.2
  3.2 0.9 copy-done.2
  4.1 0.0 copy-start.3
  4.1 0.9 copy-done.3
  5.0 0.0 copy-start.4
  5.0 0.7 copy-done.4
  5.7 0.0 copy-start.5
  5.7 0.7 copy-done.5
  6.4 0.0 copy-start.6
  6.4 0.7 copy-done.6
  7.1 0.0 copy-start.7
  7.1 0.7 copy-done.7
  7.7 0.0 copy-start.8
  7.7 0.7 copy-done.8
  8.4 84.7 %shard_map.104 = (bf16[32,32]{1,0:T(8,128)(2,1)S(1)}, f32[4,32]{1,0:T(4,128)S(1)}) custom-call(bf16[64,2048]{1,0:T(8,128)(2,1)S(1)} %bitcast.7, f32[1,2048]{1,0:T(1,128)S(1)} %bitcast.10, bf16[32,2048]{1,0:T(8,128)(2,1)S(1)} %bitcast.8, bf16[32,2048]{1,0:T(8,128)(2,1)S(1)} %bitcast.9, bf16[2048,512]{1,0:T(8,128)(2,1)S(1)} %copy-done, f32[1,32]{1,0:T(1,128)S(1)} %bitcast.12, ...), custom_call_target="tpu_custom_call" | custom-call | tf_op jit(solution)/shard_map/pallas_call | solution.py:321
  93.1 0.6 copy.13
  93.7 0.6 copy.14
Async XLA Ops:
  0.6 1.6 %copy-start = (bf16[2048,512]{1,0:T(8,128)(2,1)S(1)}, bf16[2048,512]{1,0:T(8,128)(2,1)}, u32[]{:S(2)}) copy-start(bf16[2048,512]{1,0:T(8,128)(2,1)} %wv_ref.1) | copy-start | bytes 6291460
  2.2 0.9 %copy-start.1 = (bf16[2048,64]{0,1:T(8,128)(2,1)S(1)}, bf16[2048,64]{0,1:T(8,128)(2,1)}, u32[]{:S(2)}) copy-start(bf16[2048,64]{0,1:T(8,128)(2,1)} %param.9) | copy-start | bytes 786436
  3.2 0.9 copy-start.2
  4.1 0.9 copy-start.3
  5.0 0.7 copy-start.4
  5.7 0.7 copy-start.5
  6.4 0.7 copy-start.6
  7.1 0.7 copy-start.7
  7.7 0.7 copy-start.8

commit v2 on v1

v2 whole, which is shorter than its diff:
```python
import functools

import jax
import jax.numpy as jnp
from jax import lax
from jax.experimental import pallas as pl
from jax.experimental.pallas import tpu as pltpu
from jax.sharding import PartitionSpec as P

MESH = pl.DeviceIdType.MESH
EPS = 1e-06
GATE_NORM = 16.0
KEY_CHANNELS = 256
N_SP, N_TP, N_Z = 16, 32, 16
SPAN, FEATS, VALS, CH = 2048, 64, 512, 32
SUBS = 4
SUB = SPAN // SUBS
VT = 32
HEADS = 4
MODEL = N_TP * FEATS


def column_of(row):
    n = row.shape[1]
    on_diagonal = lax.broadcasted_iota(jnp.int32, (n, n), 0) == lax.broadcasted_iota(jnp.int32, (n, n), 1)
    return jnp.sum(jnp.where(on_diagonal, jnp.broadcast_to(row, (n, n)), 0.0), axis=1, keepdims=True)


def tile_of(col, group):
    out = jnp.broadcast_to(col[0:8], (8, 128))
    for a in range(1, 4):
        out = jnp.where(group == a, jnp.broadcast_to(col[8 * a : 8 * a + 8], (8, 128)), out)
    return out


def kernel(
    x_hbm, gain_hbm, wk_hbm, wd_hbm, wv_hbm, bias_hbm, drift_hbm, q_hbm, og_hbm,
    state_ref, read_ref,
    xt, gain_ref, wk_ref, wd_ref, wv_ref, bias_ref, drift_ref, q_ref, og_ref,
    wt, acc, squares, msg, got, decay_msg, decay_got, read_msg, read_got, sq_msg, sq_got,
    in_sem, ring_send, ring_recv, pair_send, pair_recv,
    p_send, p_recv, d_send, d_recv, r_send, r_recv, s_send, s_recv,
):
    j = lax.axis_index("sp")
    t = lax.axis_index("tp")
    z, k = t // 2, t % 2
    sibling = 2 * z + 1 - k
    up = 2 * lax.rem(z + 1, N_Z) + k
    down = 2 * lax.rem(z + N_Z - 1, N_Z) + k

    barrier = pltpu.get_barrier_semaphore()
    for other in (sibling, up, down):
        pl.semaphore_signal(barrier, inc=1, device_id=(j, other), device_id_type=MESH)

    @pl.loop(1, N_SP)
    def _(o):
        pl.semaphore_signal(barrier, inc=1, device_id=(lax.rem(j + o, N_SP), t), device_id_type=MESH)

    def rows_of(src_z, core):
        return pl.ds(pl.multiple_of((2 * src_z + core) * FEATS, FEATS), FEATS)

    def lanes_of(sub):
        return pl.ds(sub * SUB, SUB)

    loads = [
        pltpu.make_async_copy(src, dst, in_sem.at[i])
        for i, (src, dst) in enumerate(
            [
                (x_hbm, xt.at[rows_of(z, k), :]), (gain_hbm, gain_ref), (wk_hbm, wk_ref), (wd_hbm, wd_ref),
                (wv_hbm, wv_ref), (bias_hbm, bias_ref), (drift_hbm, drift_ref), (q_hbm, q_ref), (og_hbm, og_ref),
            ]
        )
    ]
    for load in loads:
        load.start()

    def ring(way, sub, s):
        src_z = lax.rem(z - (s - 1) + 2 * N_Z, N_Z) if way == 0 else lax.rem(z + (s - 1), N_Z)
        place = xt.at[rows_of(src_z, k), lanes_of(sub)]
        return pltpu.make_async_remote_copy(
            src_ref=place, dst_ref=place,
            send_sem=ring_send.at[way, sub, s], recv_sem=ring_recv.at[way, sub, s],
            device_id=(j, up if way == 0 else down), device_id_type=MESH,
        )

    def pair(src_z, sub, slot):
        place = xt.at[rows_of(src_z, k), lanes_of(sub)]
        return pltpu.make_async_remote_copy(
            src_ref=place, dst_ref=place,
            send_sem=pair_send.at[slot, sub], recv_sem=pair_recv.at[slot, sub],
            device_id=(j, sibling), device_id_type=MESH,
        )

    def above(s):
        return lax.rem(z + s, N_Z)

    def below(s):
        return lax.rem(z - s + 2 * N_Z, N_Z)

    def long_way(sub):
        return 0 if sub >= SUBS // 2 else 1

    order = list(reversed(range(SUBS)))

    loads[0].wait()
    pl.semaphore_wait(barrier, 3 + N_SP - 1)
    for sub in order:
        for way in range(2):
            ring(way, sub, 1).start()
    for sub in order:
        pair(z, sub, 0).start()
    for load in loads[1:]:
        load.wait()

    gain = gain_ref[...]
    wt[VALS : VALS + CH, :] = (wk_ref[...].astype(jnp.float32) * gain).astype(jnp.bfloat16)
    wt[VALS + CH : VALS + 2 * CH, :] = (wd_ref[...].astype(jnp.float32) * gain).astype(jnp.bfloat16)

    def feats_of(src_z):
        return pl.ds(pl.multiple_of(src_z * 2 * FEATS, 2 * FEATS), 2 * FEATS)

    def prepare(src_z):
        feats = feats_of(src_z)
        wt[0:VALS, feats] = (wv_ref[feats, :].astype(jnp.float32).T * gain_ref[:, feats]).astype(jnp.bfloat16)

    def compute(sub, sources, first=False):
        lanes = lanes_of(sub)
        total = None
        sq = None
        for src in sources:
            x = xt[feats_of(src), lanes]
            term = jnp.dot(wt[:, feats_of(src)], x, preferred_element_type=jnp.float32)
            total = term if total is None else total + term
            xf = x.astype(jnp.float32)
            part = jnp.sum((xf * xf).reshape(2 * FEATS // 8, 8, SUB), axis=0)
            sq = part if sq is None else sq + part
        if first:
            acc[:, lanes] = total
            squares[:, lanes] = sq
        else:
            acc[:, lanes] += total
            squares[:, lanes] += sq

    prepare(z)

    @pl.loop(1, 8)
    def _(s):
        for at, sub in enumerate(order):
            long = long_way(sub)
            ring(long, sub, s).wait_recv()
            ring(long, sub, s + 1).start()
            pair(below(s) if long == 0 else above(s), sub, s + 8 * long).start()
            ring(1 - long, sub, s).wait_recv()

            @pl.when(s < 7)
            def _():
                ring(1 - long, sub, s + 1).start()

            pair(above(s) if long == 0 else below(s), sub, s + 8 * (1 - long)).start()
            if at == 0:
                prepare(below(s))
            if at == 1:
                prepare(above(s))

            @pl.when(s > 1)
            def _():
                pair(below(s - 1), sub, s - 1).wait_recv()
                pair(above(s - 1), sub, 7 + s).wait_recv()
                compute(sub, [below(s - 1), above(s - 1)])

            @pl.when(s == 1)
            def _():
                pair(z, sub, 0).wait_recv()
                compute(sub, [z], True)

    prepare(below(8))
    for sub in order:
        pair(below(7), sub, 7).wait_recv()
        pair(above(7), sub, 15).wait_recv()
        compute(sub, [below(7), above(7)])
        ring(long_way(sub), sub, 8).wait_recv()
        pair(below(8), sub, 8).start()

    group = lax.broadcasted_iota(jnp.int32, (8, 128), 1) // VT
    bias = column_of(bias_ref[...])
    q_tile = tile_of(column_of(q_ref[...].astype(jnp.float32)) * KEY_CHANNELS ** (-0.5), group)
    after = lax.broadcasted_iota(jnp.int32, (128, 128), 0) > lax.broadcasted_iota(jnp.int32, (128, 128), 1)
    after = jnp.where(after, 1.0, 0.0)

    def to_sp(o, source, target, send, recv):
        to = lax.rem(j + o, N_SP)
        return pltpu.make_async_remote_copy(
            src_ref=source if len(source.shape) == 2 else source.at[to], dst_ref=target.at[j],
            send_sem=send.at[o], recv_sem=recv.at[o], device_id=(to, t), device_id_type=MESH,
        )

    def decays(o):
        return to_sp(o, decay_msg, decay_got, d_send, d_recv)

    def exchange(o):
        return to_sp(o, msg, got, p_send, p_recv)

    run = jnp.zeros((CH, 1), jnp.float32)
    partial = jnp.zeros((CH, VALS), jnp.float32)
    blocks = SUB // 128
    for sub in order:
        lanes = lanes_of(sub)
        pair(below(8), sub, 8).wait_recv()
        compute(sub, [below(8)])
        inverse = lax.rsqrt(jnp.sum(squares[:, lanes], axis=0, keepdims=True) * (1.0 / MODEL) + EPS)
        gate = (acc[VALS + CH : VALS + 2 * CH, lanes] * inverse).astype(jnp.bfloat16).astype(jnp.float32)
        key = (acc[VALS : VALS + CH, lanes] * inverse).astype(jnp.bfloat16).astype(jnp.float32)
        u = gate + bias + drift_ref[:, lanes]
        log_decay = (jnp.minimum(u, 0.0) - jnp.log1p(jnp.exp(-jnp.abs(u)))) * (1.0 / GATE_NORM)
        stacked = jnp.concatenate([log_decay[:, 128 * b : 128 * b + 128] for b in range(blocks)], axis=0)
        local = jnp.dot(stacked, after, precision=lax.Precision.HIGHEST, preferred_element_type=jnp.float32)
        sums = jnp.sum(stacked, axis=1, keepdims=True)
        pieces = [None] * blocks
        for b in reversed(range(blocks)):
            rest = local[CH * b : CH * b + CH] + run
            pieces[b] = (key[:, 128 * b : 128 * b + 128] * jnp.exp(rest)).astype(jnp.bfloat16)
            run = run + sums[CH * b : CH * b + CH]
        if sub == 0:
            decay_msg[...] = tile_of(run, group)

            @pl.loop(1, N_SP)
            def _(o):
                decays(o).start()

        weighted = jnp.concatenate(pieces, axis=1)
        value = (acc[0:VALS, lanes] * inverse).astype(jnp.bfloat16)
        partial = partial + lax.dot_general(
            weighted, value, (((1,), (1,)), ((), ())), preferred_element_type=jnp.float32
        )

    for c in range(4):
        quarter = [partial[8 * a : 8 * a + 8, 128 * c : 128 * c + 128] for a in range(4)]
        for d in range(4):
            out = None
            for a in range(4):
                shift = (VT * (a - d)) % 128
                moved = quarter[a] if shift == 0 else pltpu.roll(quarter[a], shift, 1)
                out = moved if out is None else jnp.where(group == a, moved, out)
            msg[4 * c + d] = out

    @pl.loop(1, N_SP)
    def _(o):
        exchange(o).start()

    got[j] = msg[j]
    decay_got[j] = decay_msg[...]

    @pl.loop(1, N_SP)
    def _(o):
        decays(o).wait_recv()

    later = jnp.zeros((8, 128), jnp.float32)
    factors = [None] * N_SP
    for i in reversed(range(N_SP)):
        factors[i] = jnp.exp(later)
        later = later + decay_got[i]

    @pl.loop(1, N_SP)
    def _(o):
        exchange(o).wait_recv()

    state = factors[0] * got[0]
    for i in range(1, N_SP):
        state = state + factors[i] * got[i]
    read_msg[...] = jnp.sum(q_tile * state, axis=0, keepdims=True)

    def tell(o):
        return pltpu.make_async_remote_copy(
            src_ref=read_msg, dst_ref=read_got.at[t], send_sem=r_send.at[o], recv_sem=r_recv.at[o],
            device_id=(j, lax.rem(t + o, N_TP)), device_id_type=MESH,
        )

    @pl.loop(0, N_TP - 1)
    def _(i):
        tell(lax.rem(i + N_TP // 2 - 1, N_TP - 1) + 1).start()

    read_got[t] = read_msg[...]
    state_ref[...] = jnp.concatenate([state[:, VT * a : VT * a + VT] for a in range(4)], axis=0).astype(jnp.bfloat16)

    @pl.loop(1, 8)
    def _(s):
        for sub in range(SUBS):
            for way in range(2):
                ring(way, sub, s).wait_send()
            pair(below(s), sub, s).wait_send()
            pair(above(s), sub, 8 + s).wait_send()

    for sub in range(SUBS):
        ring(long_way(sub), sub, 8).wait_send()
        pair(z, sub, 0).wait_send()
        pair(below(8), sub, 8).wait_send()

    @pl.loop(1, N_SP)
    def _(o):
        exchange(o).wait_send()
        decays(o).wait_send()

    @pl.loop(1, N_TP)
    def _(o):
        tell(o).wait_recv()

    lane_group = lax.broadcasted_iota(jnp.int32, (1, 128), 1) // VT
    reads = []
    sq = jnp.zeros((1, 128), jnp.float32)
    for h in range(HEADS):
        total = read_got[8 * h]
        for i in range(1, 8):
            total = total + read_got[8 * h + i]
        total = total + pltpu.roll(total, 64, 1)
        total = total + pltpu.roll(total, 32, 1)
        reads.append(total)
        own = jnp.sum(jnp.where(lane_group == 0, total * total, 0.0), axis=1, keepdims=True)
        sq = jnp.where(lane_group == h, jnp.broadcast_to(own, (1, 128)), sq)
    sq_msg[...] = sq

    def share(o):
        return to_sp(o, sq_msg, sq_got, s_send, s_recv)

    @pl.loop(1, N_SP)
    def _(o):
        share(o).start()

    sq_got[j] = sq_msg[...]

    @pl.loop(1, N_TP)
    def _(o):
        tell(o).wait_send()

    @pl.loop(1, N_SP)
    def _(o):
        share(o).wait_recv()

    whole = sq_got[0]
    for i in range(1, N_SP):
        whole = whole + sq_got[i]
    scale = lax.rsqrt(whole * (1.0 / VALS) + EPS)
    for h in range(HEADS):
        factor = scale[:, VT * h : VT * h + VT]
        read_ref[h : h + 1, :] = reads[h][:, 0:VT] * factor * og_ref[h : h + 1, :]

    @pl.loop(1, N_SP)
    def _(o):
        share(o).wait_send()


def body(tokens, norm_gain, w_key, w_decay, w_value, decay_bias, gate_drift, queries, out_gain):
    dma = pltpu.SemaphoreType.DMA
    vmem = pl.BlockSpec(memory_space=pltpu.VMEM)
    f32, bf16 = jnp.float32, jnp.bfloat16
    return pl.pallas_call(
        kernel,
        out_shape=(jax.ShapeDtypeStruct((CH, VT), bf16), jax.ShapeDtypeStruct((HEADS, VT), f32)),
        in_specs=[pl.BlockSpec(memory_space=pl.ANY)] * 9,
        out_specs=(vmem, vmem),
        scratch_shapes=[
            pltpu.VMEM((MODEL, SPAN), bf16),
            pltpu.VMEM((1, MODEL), f32),
            pltpu.VMEM((CH, MODEL), bf16),
            pltpu.VMEM((CH, MODEL), bf16),
            pltpu.VMEM((MODEL, VALS), bf16),
            pltpu.VMEM((1, CH), f32),
            pltpu.VMEM((1, SPAN), f32),
            pltpu.VMEM((1, CH), bf16),
            pltpu.VMEM((HEADS, VT), f32),
            pltpu.VMEM((VALS + 2 * CH, MODEL), bf16),
            pltpu.VMEM((VALS + 2 * CH, SPAN), f32),
            pltpu.VMEM((8, SPAN), f32),
            pltpu.VMEM((N_SP, 8, 128), f32),
            pltpu.VMEM((N_SP, 8, 128), f32),
            pltpu.VMEM((8, 128), f32),
            pltpu.VMEM((N_SP, 8, 128), f32),
            pltpu.VMEM((1, 128), f32),
            pltpu.VMEM((N_TP, 1, 128), f32),
            pltpu.VMEM((1, 128), f32),
            pltpu.VMEM((N_SP, 1, 128), f32),
            dma((9,)), dma((2, SUBS, 9)), dma((2, SUBS, 9)), dma((16, SUBS)), dma((16, SUBS)),
            dma((N_SP,)), dma((N_SP,)), dma((N_SP,)), dma((N_SP,)), dma((N_TP,)), dma((N_TP,)), dma((N_SP,)), dma((N_SP,)),
        ],
        compiler_params=pltpu.CompilerParams(
            collective_id=0, has_side_effects=True, vmem_limit_bytes=67043328
        ),
    )(
        tokens.T, norm_gain.reshape(1, MODEL), w_key.T, w_decay.T, w_value, decay_bias.reshape(1, CH),
        gate_drift.reshape(1, SPAN), queries.reshape(1, CH), out_gain,
    )


def solution(mesh):
    return jax.shard_map(
        body,
        mesh=mesh,
        in_specs=(
            P("sp", "tp"), P(), P(None, "tp"), P(None, "tp"), P(), P("tp"), P("sp"), P("tp"), P(None, "sp"),
        ),
        out_specs=(P("tp", "sp"), P(None, "sp")),
        check_vma=False,
    )
```

time: 94.7 us -> 87.6 us (0.925)
  local copies, waits for them, and re-layouts: 8.9 us -> 2.53 us
    unnamed x20 -> x2, local copies, waits for them, and re-layouts: 8.9 us -> 2.53 us
where the time goes in v2:
time: 87.6 us; the launch traced here: 87.4 us
  Pallas kernels  84.2 us (96%)
  local copies, waits for them, and re-layouts  2.53 us (3%)
    pallas_call x1, Pallas kernels, body(): pl.pallas_call(kernel, out_shape=(jax.ShapeDtypeStruct((CH, VT), bf16), j...  84.2 us
    unnamed x2, local copies, waits for them, and re-layouts  2.53 us

profile of v2, /device:TPU:1, one launch (start us, length us, event | category | flops | bytes accessed | tf_op | source)
XLA Modules:
  0.0 87.4 jit_solution(5868600346769857971)
XLA Ops:
  0.6 84.2 %shard_map.104 = (bf16[32,32]{1,0:T(8,128)(2,1)}, f32[4,32]{1,0:T(4,128)}) custom-call(bf16[64,2048]{1,0:T(8,128)(2,1)} %bitcast.7, f32[1,2048]{1,0:T(1,128)} %bitcast.10, bf16[32,2048]{1,0:T(8,128)(2,1)} %bitcast.8, bf16[32,2048]{1,0:T(8,128)(2,1)} %bitcast.9, bf16[2048,512]{1,0:T(8,128)(2,1)} %wv_hbm.1, f32[1,32]{1,0:T(1,128)} %bitcast.12, ...), custom_call_target="tpu_custom_call" | custom-call | tf_op jit(solution)/shard_map/pallas_call | solution.py:355
  84.8 1.3 %copy.13 = bf16[32,32]{1,0:T(8,128)(2,1)} copy(bf16[32,32]{1,0:T(8,128)(2,1)} %get-tuple-element.4) | data formatting | bytes 4096
  86.1 1.2 %copy.14 = f32[4,32]{1,0:T(4,128)} copy(f32[4,32]{1,0:T(4,128)} %get-tuple-element.5) | data formatting | bytes 1024

commit v3 on v2

--- a/solution.py
+++ b/solution.py
@@ -20,6 +20,14 @@
 MODEL = N_TP * FEATS
 
 
+def hops(step, size):
+    return min(step, size - step)
+
+
+SP_ORDER = sorted(range(1, N_SP), key=lambda o: -(hops(o // 4, 4) + hops(o % 4, 4)))
+TP_ORDER = sorted(range(1, N_TP), key=lambda o: -hops(o // 2, N_Z))
+
+
 def column_of(row):
     n = row.shape[1]
     on_diagonal = lax.broadcasted_iota(jnp.int32, (n, n), 0) == lax.broadcasted_iota(jnp.int32, (n, n), 1)
@@ -35,10 +43,10 @@
 
 def kernel(
     x_hbm, gain_hbm, wk_hbm, wd_hbm, wv_hbm, bias_hbm, drift_hbm, q_hbm, og_hbm,
-    state_ref, read_ref,
+    out_ref,
     xt, gain_ref, wk_ref, wd_ref, wv_ref, bias_ref, drift_ref, q_ref, og_ref,
     wt, acc, squares, msg, got, decay_msg, decay_got, read_msg, read_got, sq_msg, sq_got,
-    in_sem, ring_send, ring_recv, pair_send, pair_recv,
+    near_sem, in_sem, ring_send, ring_recv, pair_send, pair_recv,
     p_send, p_recv, d_send, d_recv, r_send, r_recv, s_send, s_recv,
 ):
     j = lax.axis_index("sp")
@@ -51,10 +59,15 @@
     barrier = pltpu.get_barrier_semaphore()
     for other in (sibling, up, down):
         pl.semaphore_signal(barrier, inc=1, device_id=(j, other), device_id_type=MESH)
-
-    @pl.loop(1, N_SP)
-    def _(o):
-        pl.semaphore_signal(barrier, inc=1, device_id=(lax.rem(j + o, N_SP), t), device_id_type=MESH)
+    y, x = j // 4, j % 4
+
+    def at_sp(dy, dx):
+        return lax.rem(y + dy, 4) * 4 + lax.rem(x + dx, 4)
+
+    beside = (at_sp(0, 1), at_sp(0, 3))
+    across = (at_sp(1, 0), at_sp(3, 0))
+    for other in beside + across:
+        pl.semaphore_signal(barrier, inc=1, device_id=(other, t), device_id_type=MESH)
 
     def rows_of(src_z, core):
         return pl.ds(pl.multiple_of((2 * src_z + core) * FEATS, FEATS), FEATS)
@@ -103,12 +116,18 @@
     order = list(reversed(range(SUBS)))
 
     loads[0].wait()
-    pl.semaphore_wait(barrier, 3 + N_SP - 1)
+    pl.semaphore_wait(barrier, 7)
     for sub in order:
         for way in range(2):
             ring(way, sub, 1).start()
     for sub in order:
         pair(z, sub, 0).start()
+
+    def pass_on(phase, others):
+        for other in others:
+            pl.semaphore_signal(near_sem.at[phase], inc=1, device_id=(other, t), device_id_type=MESH)
+
+    pass_on(0, beside)
     for load in loads[1:]:
         load.wait()
 
@@ -173,6 +192,13 @@
                 pair(z, sub, 0).wait_recv()
                 compute(sub, [z], True)
 
+        for phase in range(3):
+            @pl.when(s == phase + 2)
+            def _():
+                pl.semaphore_wait(near_sem.at[phase], 2)
+                if phase < 2:
+                    pass_on(phase + 1, across)
+
     prepare(below(8))
     for sub in order:
         pair(below(7), sub, 7).wait_recv()
@@ -184,11 +210,12 @@
     group = lax.broadcasted_iota(jnp.int32, (8, 128), 1) // VT
     bias = column_of(bias_ref[...])
     q_tile = tile_of(column_of(q_ref[...].astype(jnp.float32)) * KEY_CHANNELS ** (-0.5), group)
-    after = lax.broadcasted_iota(jnp.int32, (128, 128), 0) > lax.broadcasted_iota(jnp.int32, (128, 128), 1)
-    after = jnp.where(after, 1.0, 0.0)
+    row_at = lax.broadcasted_iota(jnp.int32, (128, 256), 0)
+    col_at = lax.broadcasted_iota(jnp.int32, (128, 256), 1)
+    summing = jnp.where((row_at > col_at) | (col_at >= 128), 1.0, 0.0).astype(jnp.bfloat16)
 
     def to_sp(o, source, target, send, recv):
-        to = lax.rem(j + o, N_SP)
+        to = at_sp(o // 4, o % 4)
         return pltpu.make_async_remote_copy(
             src_ref=source if len(source.shape) == 2 else source.at[to], dst_ref=target.at[j],
             send_sem=send.at[o], recv_sem=recv.at[o], device_id=(to, t), device_id_type=MESH,
@@ -200,35 +227,45 @@
     def exchange(o):
         return to_sp(o, msg, got, p_send, p_recv)
 
-    run = jnp.zeros((CH, 1), jnp.float32)
+    run = jnp.zeros((CH, 128), jnp.float32)
     partial = jnp.zeros((CH, VALS), jnp.float32)
     blocks = SUB // 128
     for sub in order:
         lanes = lanes_of(sub)
         pair(below(8), sub, 8).wait_recv()
-        compute(sub, [below(8)])
-        inverse = lax.rsqrt(jnp.sum(squares[:, lanes], axis=0, keepdims=True) * (1.0 / MODEL) + EPS)
-        gate = (acc[VALS + CH : VALS + 2 * CH, lanes] * inverse).astype(jnp.bfloat16).astype(jnp.float32)
-        key = (acc[VALS : VALS + CH, lanes] * inverse).astype(jnp.bfloat16).astype(jnp.float32)
+        last = xt[feats_of(below(8)), lanes]
+        last_w = wt[:, feats_of(below(8))]
+        last_f = last.astype(jnp.float32)
+        sq = squares[:, lanes] + jnp.sum((last_f * last_f).reshape(2 * FEATS // 8, 8, SUB), axis=0)
+        inverse = lax.rsqrt(jnp.sum(sq, axis=0, keepdims=True) * (1.0 / MODEL) + EPS)
+        both = acc[VALS : VALS + 2 * CH, lanes] + jnp.dot(last_w[VALS:], last, preferred_element_type=jnp.float32)
+        both = (both * inverse).astype(jnp.bfloat16).astype(jnp.float32)
+        key, gate = both[:CH], both[CH:]
         u = gate + bias + drift_ref[:, lanes]
         log_decay = (jnp.minimum(u, 0.0) - jnp.log1p(jnp.exp(-jnp.abs(u)))) * (1.0 / GATE_NORM)
         stacked = jnp.concatenate([log_decay[:, 128 * b : 128 * b + 128] for b in range(blocks)], axis=0)
-        local = jnp.dot(stacked, after, precision=lax.Precision.HIGHEST, preferred_element_type=jnp.float32)
-        sums = jnp.sum(stacked, axis=1, keepdims=True)
+        high = stacked.astype(jnp.bfloat16)
+        left = stacked - high.astype(jnp.float32)
+        mid = left.astype(jnp.bfloat16)
+        low = (left - mid.astype(jnp.float32)).astype(jnp.bfloat16)
+        summed = (
+            jnp.dot(low, summing, preferred_element_type=jnp.float32)
+            + jnp.dot(mid, summing, preferred_element_type=jnp.float32)
+            + jnp.dot(high, summing, preferred_element_type=jnp.float32)
+        )
         pieces = [None] * blocks
         for b in reversed(range(blocks)):
-            rest = local[CH * b : CH * b + CH] + run
+            rest = summed[CH * b : CH * b + CH, 0:128] + run
             pieces[b] = (key[:, 128 * b : 128 * b + 128] * jnp.exp(rest)).astype(jnp.bfloat16)
-            run = run + sums[CH * b : CH * b + CH]
+            run = run + summed[CH * b : CH * b + CH, 128:256]
         if sub == 0:
             decay_msg[...] = tile_of(run, group)
-
-            @pl.loop(1, N_SP)
-            def _(o):
+            for o in SP_ORDER:
                 decays(o).start()
 
         weighted = jnp.concatenate(pieces, axis=1)
-        value = (acc[0:VALS, lanes] * inverse).astype(jnp.bfloat16)
+        value = acc[0:VALS, lanes] + jnp.dot(last_w[:VALS], last, preferred_element_type=jnp.float32)
+        value = (value * inverse).astype(jnp.bfloat16)
         partial = partial + lax.dot_general(
             weighted, value, (((1,), (1,)), ((), ())), preferred_element_type=jnp.float32
         )
@@ -243,15 +280,13 @@
                 out = moved if out is None else jnp.where(group == a, moved, out)
             msg[4 * c + d] = out
 
-    @pl.loop(1, N_SP)
-    def _(o):
+    for o in SP_ORDER:
         exchange(o).start()
 
     got[j] = msg[j]
     decay_got[j] = decay_msg[...]
 
-    @pl.loop(1, N_SP)
-    def _(o):
+    for o in SP_ORDER:
         decays(o).wait_recv()
 
     later = jnp.zeros((8, 128), jnp.float32)
@@ -260,8 +295,7 @@
         factors[i] = jnp.exp(later)
         later = later + decay_got[i]
 
-    @pl.loop(1, N_SP)
-    def _(o):
+    for o in SP_ORDER:
         exchange(o).wait_recv()
 
     state = factors[0] * got[0]
@@ -272,15 +306,14 @@
     def tell(o):
         return pltpu.make_async_remote_copy(
             src_ref=read_msg, dst_ref=read_got.at[t], send_sem=r_send.at[o], recv_sem=r_recv.at[o],
-            device_id=(j, lax.rem(t + o, N_TP)), device_id_type=MESH,
-        )
-
-    @pl.loop(0, N_TP - 1)
-    def _(i):
-        tell(lax.rem(i + N_TP // 2 - 1, N_TP - 1) + 1).start()
+            device_id=(j, 2 * lax.rem(z + o // 2, N_Z) + lax.rem(k + o % 2, 2)), device_id_type=MESH,
+        )
+
+    for o in TP_ORDER:
+        tell(o).start()
 
     read_got[t] = read_msg[...]
-    state_ref[...] = jnp.concatenate([state[:, VT * a : VT * a + VT] for a in range(4)], axis=0).astype(jnp.bfloat16)
+    out_ref[0:8, :] = state
 
     @pl.loop(1, 8)
     def _(s):
@@ -295,13 +328,11 @@
         pair(z, sub, 0).wait_send()
         pair(below(8), sub, 8).wait_send()
 
-    @pl.loop(1, N_SP)
-    def _(o):
+    for o in SP_ORDER:
         exchange(o).wait_send()
         decays(o).wait_send()
 
-    @pl.loop(1, N_TP)
-    def _(o):
+    for o in TP_ORDER:
         tell(o).wait_recv()
 
     lane_group = lax.broadcasted_iota(jnp.int32, (1, 128), 1) // VT
@@ -321,18 +352,15 @@
     def share(o):
         return to_sp(o, sq_msg, sq_got, s_send, s_recv)
 
-    @pl.loop(1, N_SP)
-    def _(o):
+    for o in SP_ORDER:
         share(o).start()
 
     sq_got[j] = sq_msg[...]
 
-    @pl.loop(1, N_TP)
-    def _(o):
+    for o in TP_ORDER:
         tell(o).wait_send()
 
-    @pl.loop(1, N_SP)
-    def _(o):
+    for o in SP_ORDER:
         share(o).wait_recv()
 
     whole = sq_got[0]
@@ -341,22 +369,27 @@
     scale = lax.rsqrt(whole * (1.0 / VALS) + EPS)
     for h in range(HEADS):
         factor = scale[:, VT * h : VT * h + VT]
-        read_ref[h : h + 1, :] = reads[h][:, 0:VT] * factor * og_ref[h : h + 1, :]
-
-    @pl.loop(1, N_SP)
-    def _(o):
+        out_ref[8 + h : 9 + h, 0:VT] = reads[h][:, 0:VT] * factor * og_ref[h : h + 1, :]
+
+    for o in SP_ORDER:
         share(o).wait_send()
+
+
+def unpack(packed_ref, state_ref, read_ref):
+    state = packed_ref[0:8, :]
+    state_ref[...] = jnp.concatenate([state[:, VT * a : VT * a + VT] for a in range(4)], axis=0).astype(jnp.bfloat16)
+    read_ref[...] = packed_ref[8 : 8 + HEADS, 0:VT]
 
 
 def body(tokens, norm_gain, w_key, w_decay, w_value, decay_bias, gate_drift, queries, out_gain):
     dma = pltpu.SemaphoreType.DMA
     vmem = pl.BlockSpec(memory_space=pltpu.VMEM)
     f32, bf16 = jnp.float32, jnp.bfloat16
-    return pl.pallas_call(
+    packed = pl.pallas_call(
         kernel,
-        out_shape=(jax.ShapeDtypeStruct((CH, VT), bf16), jax.ShapeDtypeStruct((HEADS, VT), f32)),
+        out_shape=jax.ShapeDtypeStruct((16, 128), f32),
         in_specs=[pl.BlockSpec(memory_space=pl.ANY)] * 9,
-        out_specs=(vmem, vmem),
+        out_specs=vmem,
         scratch_shapes=[
             pltpu.VMEM((MODEL, SPAN), bf16),
             pltpu.VMEM((1, MODEL), f32),
@@ -378,7 +411,7 @@
             pltpu.VMEM((N_TP, 1, 128), f32),
             pltpu.VMEM((1, 128), f32),
             pltpu.VMEM((N_SP, 1, 128), f32),
-            dma((9,)), dma((2, SUBS, 9)), dma((2, SUBS, 9)), dma((16, SUBS)), dma((16, SUBS)),
+            pltpu.SemaphoreType.REGULAR((3,)), dma((9,)), dma((2, SUBS, 9)), dma((2, SUBS, 9)), dma((16, SUBS)), dma((16, SUBS)),
             dma((N_SP,)), dma((N_SP,)), dma((N_SP,)), dma((N_SP,)), dma((N_TP,)), dma((N_TP,)), dma((N_SP,)), dma((N_SP,)),
         ],
         compiler_params=pltpu.CompilerParams(
@@ -388,6 +421,12 @@
         tokens.T, norm_gain.reshape(1, MODEL), w_key.T, w_decay.T, w_value, decay_bias.reshape(1, CH),
         gate_drift.reshape(1, SPAN), queries.reshape(1, CH), out_gain,
     )
+    return pl.pallas_call(
+        unpack,
+        out_shape=(jax.ShapeDtypeStruct((CH, VT), bf16), jax.ShapeDtypeStruct((HEADS, VT), f32)),
+        in_specs=[vmem],
+        out_specs=(vmem, vmem),
+    )(packed)
 
 
 def solution(mesh):

time: 87.6 us -> 83.7 us (0.955)
  local copies, waits for them, and re-layouts: 2.53 us -> 0 us
  Pallas kernels: 84.2 us -> 82.9 us
    unnamed x2 -> x0, local copies, waits for them, and re-layouts: 2.53 us -> none
    pallas_call x1 -> x2, Pallas kernels: 84.2 us -> 82.9 us  [the longest x1 81.5 us: body(): pl.pallas_call(kernel, out_shape=jax.ShapeDtypeStruct((16, 128), f32), in...]
where the time goes in v3:
time: 83.7 us; the launch traced here: 83.5 us
  Pallas kernels  82.9 us (99%)
    pallas_call x1, Pallas kernels, body(): pl.pallas_call(kernel, out_shape=jax.ShapeDtypeStruct((16, 128), f32), in...  81.5 us

profile of v3, /device:TPU:1, one launch (start us, length us, event | category | flops | bytes accessed | tf_op | source)
XLA Modules:
  0.0 83.5 jit_solution(4535026196157135491)
XLA Ops:
  0.6 81.5 %shard_map.104.packed_ref = f32[16,128]{1,0:T(8,128)} custom-call(bf16[64,2048]{1,0:T(8,128)(2,1)} %bitcast.7, f32[1,2048]{1,0:T(1,128)} %bitcast.10, bf16[32,2048]{1,0:T(8,128)(2,1)} %bitcast.8, bf16[32,2048]{1,0:T(8,128)(2,1)} %bitcast.9, bf16[2048,512]{1,0:T(8,128)(2,1)} %wv_hbm.1, f32[1,32]{1,0:T(1,128)} %bitcast.12, f32[1,2048]{1,0:T(1,128)} %bitcast.11, ...), custom_call_target="tpu_custom_call" | custom-call | tf_op jit(solution)/shard_map/pallas_call | solution.py:388
  82.2 1.4 %shard_map.105 = (bf16[32,32]{1,0:T(8,128)(2,1)}, f32[4,32]{1,0:T(4,128)}) custom-call(f32[16,128]{1,0:T(8,128)} %shard_map.104.packed_ref), custom_call_target="tpu_custom_call" | custom-call | tf_op jit(solution)/shard_map/pallas_call | solution.py:424

commit v4 on v0

v4 whole, which is shorter than its diff:
```python
import jax
import jax.numpy as jnp
from jax import lax
from jax.experimental import pallas as pl
from jax.experimental.pallas import tpu as pltpu
from jax.sharding import PartitionSpec as P

MESH = pl.DeviceIdType.MESH
EPS = 1e-06
GATE_NORM = 16.0
KEY_CHANNELS = 256
N_SP, N_TP, N_Z = 16, 32, 16
SPAN, FEATS, VALS, CH = 2048, 64, 512, 32
QUARTERS = 4
ROWS = SPAN // QUARTERS
NCH = QUARTERS * CH
VT = 32
HEADS = 4
MODEL = N_TP * FEATS
STEPS = 9
HIGH = lax.Precision.HIGHEST


def hops(step, size):
    return min(step, size - step)


def sp_hops(o):
    return hops(o // 4, 4) + hops(o % 4, 4)


SP_ORDER = sorted(range(1, N_SP), key=lambda o: -sp_hops(o))
TP_ORDER = sorted(range(1, N_TP), key=lambda o: -hops(o // 2, N_Z))
ALL_ORDER = sorted(range(1, 4 * N_SP), key=lambda o: -(hops(4 * (o // 16), N_Z) + sp_hops(o % 16)))


def column_of(row):
    n = row.shape[1]
    on_diagonal = lax.broadcasted_iota(jnp.int32, (n, n), 0) == lax.broadcasted_iota(jnp.int32, (n, n), 1)
    return jnp.sum(jnp.where(on_diagonal, jnp.broadcast_to(row, (n, n)), 0.0), axis=1, keepdims=True)


def lane_row(rows):
    at = lax.broadcasted_iota(jnp.int32, (VT, 128), 1)
    pick = jnp.where(lax.rem(at, VT) == lax.broadcasted_iota(jnp.int32, (VT, 128), 0), 1.0, 0.0)
    wide = jnp.dot(rows, pick, precision=HIGH, preferred_element_type=jnp.float32)
    lane = lax.broadcasted_iota(jnp.int32, (8, 128), 1) // VT
    mine = lane == lax.broadcasted_iota(jnp.int32, (8, 128), 0)
    return jnp.sum(jnp.where(mine, wide, 0.0), axis=0, keepdims=True)


def kernel(
    x_hbm, gain_hbm, wk_hbm, wd_hbm, wv_hbm, bias_hbm, drift_hbm, q_hbm, og_hbm,
    out_ref,
    xs, xt, gain_ref, wk_ref, wd_ref, wv_ref, bias_ref, drift_ref, q_ref, og_ref,
    wrel, acc, squares, small_msg, small_got, key_scr, gate_scr, msg, got, d_msg, d_got,
    read_msg, read_got, sq_msg, sq_got, st_got, turned,
    near_sem, in_sem, z_send, z_recv, f_send, c_send, c_recv, w1_send, w1_recv, w2_send, w2_recv, b_send, b_recv,
    d_send, d_recv, p_send, p_recv, r_send, r_recv, t_send, t_recv, s_send, s_recv,
):
    j = lax.axis_index("sp")
    t = lax.axis_index("tp")
    z, k = t // 2, t % 2
    quarter, i = z // 4, z % 4
    y, x = j // 4, j % 4
    sibling = 2 * z + 1 - k

    def at_sp(dy, dx):
        return lax.rem(y + dy, 4) * 4 + lax.rem(x + dx, 4)

    def ahead(dz):
        return lax.rem(z + dz, N_Z)

    barrier = pltpu.get_barrier_semaphore()
    pl.semaphore_signal(barrier, inc=1, device_id=(j, sibling), device_id_type=MESH)
    beside = (at_sp(0, 1), at_sp(0, 3))
    across = (at_sp(1, 0), at_sp(3, 0))
    for other in beside + across:
        pl.semaphore_signal(barrier, inc=1, device_id=(other, t), device_id_type=MESH)
    for dz in range(1, N_Z):
        pl.semaphore_signal(barrier, inc=1, device_id=(j, 2 * ahead(dz) + k), device_id_type=MESH)

    def rows_of(src_z, core):
        return pl.ds(pl.multiple_of((2 * src_z + core) * FEATS, FEATS), FEATS)

    def group_of(q):
        return pl.ds(pl.multiple_of(q * ROWS, ROWS), ROWS)

    my_lanes = pl.ds(pl.multiple_of(j * 128, 128), 128)

    loads = [
        pltpu.make_async_copy(src, dst, in_sem.at[n])
        for n, (src, dst) in enumerate(
            [
                (x_hbm, xs), (gain_hbm, gain_ref), (wk_hbm, wk_ref), (wd_hbm, wd_ref), (bias_hbm, bias_ref),
                (q_hbm, q_ref), (x_hbm.at[:, group_of(quarter)], xt.at[rows_of(z, k), :]),
                (wv_hbm, wv_ref), (drift_hbm, drift_ref), (og_hbm, og_ref),
            ]
        )
    ]
    for load in loads:
        load.start()
    for load in loads[:7]:
        load.wait()
    gain = gain_ref[...]
    wrel[0, 0:CH, :] = (wk_ref[...].astype(jnp.float32) * gain).astype(jnp.bfloat16)
    wrel[0, CH : 2 * CH, :] = (wd_ref[...].astype(jnp.float32) * gain).astype(jnp.bfloat16)
    small_msg[...] = jnp.zeros((2, 128), jnp.float32)
    small_msg[0:1, 0:CH] = bias_ref[...]
    small_msg[1:2, 0:CH] = q_ref[...].astype(jnp.float32) * KEY_CHANNELS ** (-0.5)
    pl.semaphore_wait(barrier, 5 + N_Z - 1)

    def pass_on(phase, others):
        for other in others:
            pl.semaphore_signal(near_sem.at[phase], inc=1, device_id=(other, t), device_id_type=MESH)

    pass_on(0, beside)

    def weights_along(n):
        return pltpu.make_async_remote_copy(
            src_ref=wrel.at[0, :, my_lanes], dst_ref=wrel.at[4 - n, :, my_lanes],
            send_sem=w1_send.at[n], recv_sem=w1_recv.at[4 - n],
            device_id=(j, 2 * ahead(4 * n) + k), device_id_type=MESH,
        )

    def weights_there(n):
        return pltpu.make_async_remote_copy(
            src_ref=wrel.at[0, :, my_lanes], dst_ref=wrel.at[n, :, my_lanes],
            send_sem=w1_send.at[n], recv_sem=w1_recv.at[n],
            device_id=(j, 2 * ahead(4 * n) + k), device_id_type=MESH,
        )

    def small_along(n):
        return pltpu.make_async_remote_copy(
            src_ref=small_msg, dst_ref=small_got.at[quarter],
            send_sem=b_send.at[n], recv_sem=b_recv.at[4 - n],
            device_id=(j, 2 * ahead(4 * n) + k), device_id_type=MESH,
        )

    def weights_across(o):
        return pltpu.make_async_remote_copy(
            src_ref=wrel.at[pl.ds(1, 3), :, my_lanes], dst_ref=wrel.at[pl.ds(1, 3), :, my_lanes],
            send_sem=w2_send.at[o], recv_sem=w2_recv.at[o],
            device_id=(at_sp(o // 4, o % 4), t), device_id_type=MESH,
        )

    def send_block(source, src_z, dst_z, sem):
        return pltpu.make_async_remote_copy(
            src_ref=source, dst_ref=xt.at[rows_of(src_z, k), :], send_sem=sem, recv_sem=z_recv.at[src_z],
            device_id=(j, 2 * dst_z + k), device_id_type=MESH,
        )

    nxt, opp, prv = lax.rem(quarter + 1, 4), lax.rem(quarter + 2, 4), lax.rem(quarter + 3, 4)
    own_sends = [
        send_block(xs.at[:, group_of(quarter)], z, ahead(1), z_send.at[0]),
        send_block(xs.at[:, group_of(quarter)], z, ahead(N_Z - 1), z_send.at[1]),
        send_block(xs.at[:, group_of(nxt)], z, 4 * nxt, z_send.at[2]),
        send_block(xs.at[:, group_of(prv)], z, 4 * prv + 3, z_send.at[3]),
        send_block(xs.at[:, group_of(opp)], z, 4 * opp + jnp.where(i >= 2, 0, 3), z_send.at[4]),
    ]
    for n in (2, 1, 3):
        weights_along(n).start()

    @pl.when(i < 3)
    def _():
        own_sends[0].start()

    @pl.when(i > 0)
    def _():
        own_sends[1].start()

    for send in own_sends[2:]:
        send.start()

    def to_core(src_z, way, n):
        place = xt.at[rows_of(src_z, k), :]
        return pltpu.make_async_remote_copy(
            src_ref=place, dst_ref=place, send_sem=c_send.at[way, n], recv_sem=c_recv.at[way, n],
            device_id=(j, sibling), device_id_type=MESH,
        )

    to_core(z, 0, STEPS).start()
    for n in (2, 1, 3):
        small_along(n).start()
    small_got[quarter] = small_msg[...]
    for load in loads[7:]:
        load.wait()

    def source(way, n):
        if n < 3:
            return lax.rem(z - (n + 1) + N_Z, N_Z) if way == 0 else ahead(n + 1)
        e = n - 3
        if e < 4:
            return 4 * prv + 3 - e if way == 0 else 4 * nxt + e
        return 4 * opp + 3 - (e - 4) if way == 0 else 4 * opp + e - 4

    def here(way, n):
        return i >= n + 1 if way == 0 else i + n + 1 <= 3

    def when_here(way, n, action):
        if n < 3:
            pl.when(here(way, n))(action)
        else:
            action()

    def onward(way, n):
        src = source(way, n)
        return send_block(xt.at[rows_of(src, k), :], src, ahead(1 if way == 0 else N_Z - 1), f_send.at[way, n])

    def goes_on(way):
        return i < 3 if way == 0 else i > 0

    def take(way, n):
        def action():
            src = source(way, n)
            place = xt.at[rows_of(src, k), :]
            pltpu.make_async_remote_copy(
                src_ref=place, dst_ref=place, send_sem=f_send.at[way, n], recv_sem=z_recv.at[src],
                device_id=(j, sibling), device_id_type=MESH,
            ).wait_recv()

            @pl.when(goes_on(way))
            def _():
                onward(way, n).start()

            to_core(src, way, n).start()

        when_here(way, n, action)

    def feats_of(src_z):
        return pl.ds(pl.multiple_of(src_z * 2 * FEATS, 2 * FEATS), 2 * FEATS)

    def compute(src_z, first=False):
        feats = feats_of(src_z)
        w = (wv_ref[feats, :].astype(jnp.float32).T * gain_ref[:, feats]).astype(jnp.bfloat16)
        block = xt[feats, :]
        term = jnp.dot(w, block, preferred_element_type=jnp.float32)
        wide = block.astype(jnp.float32)
        sq = jnp.sum((wide * wide).reshape(2 * FEATS // 8, 8, ROWS), axis=0)
        if first:
            acc[...] = term
            squares[...] = sq
        else:
            acc[...] += term
            squares[...] += sq

    def process(way, n):
        def action():
            src = source(way, n)
            to_core(src, way, n).wait_recv()
            compute(src)

        when_here(way, n, action)

    for n in range(STEPS):
        for way in range(2):
            take(way, n)
        if n == 0:
            to_core(z, 0, STEPS).wait_recv()
            compute(z, True)
        else:
            for way in range(2):
                process(way, n - 1)
        if n in (1, 2, 3):
            phase = n - 1
            pl.semaphore_wait(near_sem.at[phase], 2)
            if phase < 2:
                pass_on(phase + 1, across)
        if n == 4:
            for m in range(1, 4):
                weights_there(m).wait_recv()
            for o in SP_ORDER:
                weights_across(o).start()
    for n in range(1, 4):
        small_along(n).wait_recv()
    bias = jnp.concatenate([column_of(small_got[b, 0:1, 0:CH]) for b in range(4)], axis=0)
    q_rows = jnp.concatenate([small_got[b, 1:2, 0:CH] for b in range(4)] + [jnp.zeros((4, CH), jnp.float32)], axis=0)
    q_row = lane_row(q_rows)
    og_row = lane_row(jnp.concatenate([og_ref[...], jnp.zeros((4, VT), jnp.float32)], axis=0))
    row_at = lax.broadcasted_iota(jnp.int32, (128, 256), 0)
    col_at = lax.broadcasted_iota(jnp.int32, (128, 256), 1)
    summing = jnp.where((row_at > col_at) | (col_at >= 128), 1.0, 0.0).astype(jnp.bfloat16)
    for o in SP_ORDER:
        weights_across(o).wait_recv()
    for way in range(2):
        process(way, STEPS - 1)

    inverse = lax.rsqrt(jnp.sum(squares[...], axis=0, keepdims=True) * (1.0 / MODEL) + EPS)
    both = jnp.dot(wrel[...].reshape(4 * 2 * CH, MODEL), xt[...], preferred_element_type=jnp.float32)
    both = (both * inverse).astype(jnp.bfloat16).astype(jnp.float32)
    for m in range(4):
        b = lax.rem(quarter + m, 4)
        key_scr[b] = both[2 * CH * m : 2 * CH * m + CH]
        gate_scr[b] = both[2 * CH * m + CH : 2 * CH * m + 2 * CH]
    key = key_scr[...].reshape(NCH, ROWS)
    u = gate_scr[...].reshape(NCH, ROWS) + bias + drift_ref[:, group_of(quarter)]
    log_decay = (jnp.minimum(u, 0.0) - jnp.log1p(jnp.exp(-jnp.abs(u)))) * (1.0 / GATE_NORM)
    blocks = ROWS // 128
    stacked = jnp.concatenate([log_decay[:, 128 * b : 128 * b + 128] for b in range(blocks)], axis=0)
    high = stacked.astype(jnp.bfloat16)
    left = stacked - high.astype(jnp.float32)
    mid = left.astype(jnp.bfloat16)
    low = (left - mid.astype(jnp.float32)).astype(jnp.bfloat16)
    summed = (
        jnp.dot(low, summing, preferred_element_type=jnp.float32)
        + jnp.dot(mid, summing, preferred_element_type=jnp.float32)
        + jnp.dot(high, summing, preferred_element_type=jnp.float32)
    )
    rests = [None] * blocks
    run = jnp.zeros((NCH, 128), jnp.float32)
    for b in reversed(range(blocks)):
        rests[b] = summed[NCH * b : NCH * b + NCH, 0:128] + run
        run = run + summed[NCH * b : NCH * b + NCH, 128:256]
    d_msg[...] = run.T[0:1, :]

    def decays(o):
        return pltpu.make_async_remote_copy(
            src_ref=d_msg, dst_ref=d_got.at[4 * j + quarter], send_sem=d_send.at[o], recv_sem=d_recv.at[o],
            device_id=(at_sp((o % 16) // 4, o % 4), 2 * ahead(4 * (o // 16)) + k), device_id_type=MESH,
        )

    for o in ALL_ORDER:
        decays(o).start()
    d_got[4 * j + quarter] = d_msg[...]
    weighted = jnp.concatenate(
        [(key[:, 128 * b : 128 * b + 128] * jnp.exp(rests[b])).astype(jnp.bfloat16) for b in range(blocks)], axis=1
    )
    value = (acc[...] * inverse).astype(jnp.bfloat16)
    partial = lax.dot_general(value, weighted, (((1,), (1,)), ((), ())), preferred_element_type=jnp.float32)
    msg[...] = partial.reshape(N_SP, VT, NCH)

    def exchange(o):
        to = at_sp(o // 4, o % 4)
        return pltpu.make_async_remote_copy(
            src_ref=msg.at[to], dst_ref=got.at[j], send_sem=p_send.at[o], recv_sem=p_recv.at[o],
            device_id=(to, t), device_id_type=MESH,
        )

    for o in SP_ORDER:
        exchange(o).start()
    got[j] = msg[j]

    for way in range(2):
        for n in range(STEPS):
            def action(way=way, n=n):
                @pl.when(goes_on(way))
                def _():
                    onward(way, n).wait_send()

                to_core(source(way, n), way, n).wait_send()

            when_here(way, n, action)
    to_core(z, 0, STEPS).wait_send()

    @pl.when(i < 3)
    def _():
        own_sends[0].wait_send()

    @pl.when(i > 0)
    def _():
        own_sends[1].wait_send()

    for send in own_sends[2:]:
        send.wait_send()
    for n in range(1, 4):
        weights_along(n).wait_send()
        small_along(n).wait_send()
    for o in SP_ORDER:
        weights_across(o).wait_send()

    for o in SP_ORDER:
        exchange(o).wait_recv()
    for o in reversed(ALL_ORDER):
        decays(o).wait_recv()
    later = jnp.zeros((1, NCH), jnp.float32)
    state = jnp.zeros((VT, NCH), jnp.float32)
    for n in reversed(range(N_SP)):
        mine = later
        for g in range(4):
            piece = d_got[4 * n + g]
            mine = mine + jnp.where(g > quarter, piece, 0.0)
            later = later + piece
        state = state + jnp.exp(mine) * got[n]
    lane_head = lax.broadcasted_iota(jnp.int32, (8, 128), 1) // VT
    pick_head = jnp.where(lane_head == lax.broadcasted_iota(jnp.int32, (8, 128), 0), 1.0, 0.0)
    head_rows = lax.dot_general(
        pick_head, state * q_row, (((1,), (1,)), ((), ())), precision=HIGH, preferred_element_type=jnp.float32
    )
    read_msg[...] = lane_row(head_rows)

    def tell(o):
        return pltpu.make_async_remote_copy(
            src_ref=read_msg, dst_ref=read_got.at[t], send_sem=r_send.at[o], recv_sem=r_recv.at[o],
            device_id=(j, 2 * ahead(o // 2) + lax.rem(k + o % 2, 2)), device_id_type=MESH,
        )

    for o in TP_ORDER:
        tell(o).start()
    st_got[0] = state

    def states(n):
        return pltpu.make_async_remote_copy(
            src_ref=st_got.at[0], dst_ref=st_got.at[4 - n], send_sem=t_send.at[n], recv_sem=t_recv.at[4 - n],
            device_id=(j, 2 * ahead(4 * n) + k), device_id_type=MESH,
        )

    for n in (2, 1, 3):
        states(n).start()
    read_got[t] = read_msg[...]
    for o in SP_ORDER:
        exchange(o).wait_send()
    for o in ALL_ORDER:
        decays(o).wait_send()
    for o in TP_ORDER:
        tell(o).wait_recv()
    read = read_got[0]
    for n in range(1, N_TP):
        read = read + read_got[n]
    lane_group = lax.broadcasted_iota(jnp.int32, (1, 128), 1) // VT
    sq = jnp.zeros((1, 128), jnp.float32)
    for h in range(HEADS):
        own = jnp.sum(jnp.where(lane_group == h, read * read, 0.0), axis=1, keepdims=True)
        sq = jnp.where(lane_group == h, jnp.broadcast_to(own, (1, 128)), sq)
    sq_msg[...] = sq

    def share(o):
        return pltpu.make_async_remote_copy(
            src_ref=sq_msg, dst_ref=sq_got.at[j], send_sem=s_send.at[o], recv_sem=s_recv.at[o],
            device_id=(at_sp(o // 4, o % 4), t), device_id_type=MESH,
        )

    for o in SP_ORDER:
        share(o).start()
    sq_got[j] = sq_msg[...]
    for n in range(1, 4):
        states(n).wait_recv()
    total = st_got[0] + st_got[1] + st_got[2] + st_got[3]
    turned[...] = jnp.concatenate([total] * 4, axis=0).T
    out_ref[0:CH, :] = turned[pl.ds(pl.multiple_of(CH * quarter, CH), CH), :]
    for n in range(1, 4):
        states(n).wait_send()
    for o in TP_ORDER:
        tell(o).wait_send()
    for o in SP_ORDER:
        share(o).wait_recv()
    whole = sq_got[0]
    for n in range(1, N_SP):
        whole = whole + sq_got[n]
    out_ref[CH : CH + 1, :] = read * lax.rsqrt(whole * (1.0 / VALS) + EPS) * og_row
    for o in SP_ORDER:
        share(o).wait_send()


def unpack(packed_ref, state_ref, read_ref):
    state_ref[...] = packed_ref[0:CH, 0:VT].astype(jnp.bfloat16)
    for h in range(HEADS):
        read_ref[h : h + 1, :] = packed_ref[CH : CH + 1, VT * h : VT * h + VT]


def body(tokens, norm_gain, w_key, w_decay, w_value, decay_bias, gate_drift, queries, out_gain):
    dma = pltpu.SemaphoreType.DMA
    vmem = pl.BlockSpec(memory_space=pltpu.VMEM)
    f32, bf16 = jnp.float32, jnp.bfloat16
    packed = pl.pallas_call(
        kernel,
        out_shape=jax.ShapeDtypeStruct((CH + 8, 128), f32),
        in_specs=[pl.BlockSpec(memory_space=pl.ANY)] * 9,
        out_specs=vmem,
        scratch_shapes=[
            pltpu.VMEM((FEATS, SPAN), bf16),
            pltpu.VMEM((MODEL, ROWS), bf16),
            pltpu.VMEM((1, MODEL), f32),
            pltpu.VMEM((CH, MODEL), bf16),
            pltpu.VMEM((CH, MODEL), bf16),
            pltpu.VMEM((MODEL, VALS), bf16),
            pltpu.VMEM((1, CH), f32),
            pltpu.VMEM((1, SPAN), f32),
            pltpu.VMEM((1, CH), bf16),
            pltpu.VMEM((HEADS, VT), f32),
            pltpu.VMEM((4, 2 * CH, MODEL), bf16),
            pltpu.VMEM((VALS, ROWS), f32),
            pltpu.VMEM((8, ROWS), f32),
            pltpu.VMEM((2, 128), f32),
            pltpu.VMEM((4, 2, 128), f32),
            pltpu.VMEM((4, CH, ROWS), f32),
            pltpu.VMEM((4, CH, ROWS), f32),
            pltpu.VMEM((N_SP, VT, NCH), f32),
            pltpu.VMEM((N_SP, VT, NCH), f32),
            pltpu.VMEM((1, 128), f32),
            pltpu.VMEM((4 * N_SP, 1, 128), f32),
            pltpu.VMEM((1, 128), f32),
            pltpu.VMEM((N_TP, 1, 128), f32),
            pltpu.VMEM((1, 128), f32),
            pltpu.VMEM((N_SP, 1, 128), f32),
            pltpu.VMEM((4, VT, NCH), f32),
            pltpu.VMEM((128, 128), f32),
            pltpu.SemaphoreType.REGULAR((3,)), dma((10,)), dma((5,)), dma((N_Z,)), dma((2, STEPS)),
            dma((2, STEPS + 1)), dma((2, STEPS + 1)), dma((4,)), dma((4,)), dma((N_SP,)), dma((N_SP,)), dma((4,)), dma((4,)),
            dma((64,)), dma((64,)), dma((N_SP,)), dma((N_SP,)), dma((N_TP,)), dma((N_TP,)), dma((4,)), dma((4,)),
            dma((N_SP,)), dma((N_SP,)),
        ],
        compiler_params=pltpu.CompilerParams(
            collective_id=0, has_side_effects=True, vmem_limit_bytes=67043328
        ),
    )(
        tokens.T, norm_gain.reshape(1, MODEL), w_key.T, w_decay.T, w_value, decay_bias.reshape(1, CH),
        gate_drift.reshape(1, SPAN), queries.reshape(1, CH), out_gain,
    )
    return pl.pallas_call(
        unpack,
        out_shape=(jax.ShapeDtypeStruct((CH, VT), bf16), jax.ShapeDtypeStruct((HEADS, VT), f32)),
        in_specs=[vmem],
        out_specs=(vmem, vmem),
    )(packed)


def solution(mesh):
    return jax.shard_map(
        body,
        mesh=mesh,
        in_specs=(
            P("sp", "tp"), P(), P(None, "tp"), P(None, "tp"), P(), P("tp"), P("sp"), P("tp"), P(None, "sp"),
        ),
        out_specs=(P("tp", "sp"), P(None, "sp")),
        check_vma=False,
    )
```

time: 234 us -> 186 us (0.79)
  Pallas kernels: 0 us -> 186 us
  waiting for transfers between devices: 98.8 us -> 0 us
  other arithmetic: 58.3 us -> 0 us
  blocking collectives: 21.4 us -> 0 us
  matrix products: 19.5 us -> 0 us
  starting transfers between devices: 16.8 us -> 0 us
  between operations: 14.3 us -> 0.64 us
  local copies, waits for them, and re-layouts: 4.45 us -> 0 us
    pallas_call x0 -> x2, Pallas kernels: none -> 186 us  [the longest x1 184 us: body(): pl.pallas_call(kernel, out_shape=jax.ShapeDtypeStruct((CH + 8, 128), f32)...]
    all_gather x1 -> x0, waiting for transfers between devices: 86 us -> none  [body(): gathered = lax.all_gather(tokens, 'tp', axis=1, tiled=True)]
    another operation x4 -> x0, other arithmetic: 40.1 us -> none
    all_to_all x1 -> x0, blocking collectives: 21.4 us -> none  [copy_for_each(): return lax.all_to_all(copies, axis, split_axis=0, concat_axis=0, tiled=True)]
    dot_general x4 -> x0, matrix products: 19.5 us -> none  [the longest x1 9.21 us: body(): lax.dot_general(weighted, value_proj, (((0,), (0,)), ((), ())), preferred...]
    all_to_all x3 -> x0, starting transfers between devices: 16.8 us -> none  [the longest x1 6.65 us: body(): lax.all_to_all(partial_value[None], 'sp', split_axis=2, concat_axis=0, ti...]
    all_to_all x3 -> x0, waiting for transfers between devices: 12.2 us -> none  [the longest x1 6.47 us: body(): lax.all_to_all(partial_value[None], 'sp', split_axis=2, concat_axis=0, ti...]
    convert_element_type x1 -> x0, other arithmetic: 8.58 us -> none  [body(): normed = (rows_f32 * inverse_rms * norm_gain[None, :]).astype(jnp.bfloat16)]
  transfers between devices with their start and end apart: 4 -> 0, of which waited for: 3 -> 0; matrix products, arithmetic and copies ran while one was open for 6% -> 0% of each run, Pallas kernels for 0% -> 0%
where the time goes in v4:
time: 186 us
  Pallas kernels  186 us (100%)
    pallas_call x1, Pallas kernels, body(): pl.pallas_call(kernel, out_shape=jax.ShapeDtypeStruct((CH + 8, 128), f32)...  184 us

profile of v4, /device:TPU:1, one launch (start us, length us, event | category | flops | bytes accessed | tf_op | source)
XLA Modules:
  0.0 186.2 jit_solution(12207728921044164325)
XLA Ops:
  0.6 184.2 %shard_map.104.packed_ref = f32[40,128]{1,0:T(8,128)} custom-call(bf16[64,2048]{1,0:T(8,128)(2,1)} %bitcast.7, f32[1,2048]{1,0:T(1,128)} %bitcast.10, bf16[32,2048]{1,0:T(8,128)(2,1)} %bitcast.8, bf16[32,2048]{1,0:T(8,128)(2,1)} %bitcast.9, bf16[2048,512]{1,0:T(8,128)(2,1)} %wv_hbm.1, f32[1,32]{1,0:T(1,128)} %bitcast.12, f32[1,2048]{1,0:T(1,128)} %bitcast.11, ...), custom_call_target="tpu_custom_call" | custom-call | tf_op jit(solution)/shard_map/pallas_call | solution.py:464
  184.8 1.4 shard_map.105

commit v5 on v4

--- a/solution.py
+++ b/solution.py
@@ -18,6 +18,8 @@
 HEADS = 4
 MODEL = N_TP * FEATS
 STEPS = 9
+BEATS = 12
+WEIGHT_BEAT = 4
 HIGH = lax.Precision.HIGHEST
 
 
@@ -53,7 +55,7 @@
     x_hbm, gain_hbm, wk_hbm, wd_hbm, wv_hbm, bias_hbm, drift_hbm, q_hbm, og_hbm,
     out_ref,
     xs, xt, gain_ref, wk_ref, wd_ref, wv_ref, bias_ref, drift_ref, q_ref, og_ref,
-    wrel, acc, squares, small_msg, small_got, key_scr, gate_scr, msg, got, d_msg, d_got,
+    wrel, wvt, squares, small_msg, small_got, key_scr, gate_scr, msg, got, d_msg, d_got,
     read_msg, read_got, sq_msg, sq_got, st_got, turned,
     near_sem, in_sem, z_send, z_recv, f_send, c_send, c_recv, w1_send, w1_recv, w2_send, w2_recv, b_send, b_recv,
     d_send, d_recv, p_send, p_recv, r_send, r_recv, t_send, t_recv, s_send, s_recv,
@@ -103,8 +105,8 @@
     for load in loads[:7]:
         load.wait()
     gain = gain_ref[...]
-    wrel[0, 0:CH, :] = (wk_ref[...].astype(jnp.float32) * gain).astype(jnp.bfloat16)
-    wrel[0, CH : 2 * CH, :] = (wd_ref[...].astype(jnp.float32) * gain).astype(jnp.bfloat16)
+    wrel[0, 0] = (wk_ref[...].astype(jnp.float32) * gain).astype(jnp.bfloat16)
+    wrel[1, 0] = (wd_ref[...].astype(jnp.float32) * gain).astype(jnp.bfloat16)
     small_msg[...] = jnp.zeros((2, 128), jnp.float32)
     small_msg[0:1, 0:CH] = bias_ref[...]
     small_msg[1:2, 0:CH] = q_ref[...].astype(jnp.float32) * KEY_CHANNELS ** (-0.5)
@@ -118,14 +120,14 @@
 
     def weights_along(n):
         return pltpu.make_async_remote_copy(
-            src_ref=wrel.at[0, :, my_lanes], dst_ref=wrel.at[4 - n, :, my_lanes],
+            src_ref=wrel.at[:, 0, :, my_lanes], dst_ref=wrel.at[:, 4 - n, :, my_lanes],
             send_sem=w1_send.at[n], recv_sem=w1_recv.at[4 - n],
             device_id=(j, 2 * ahead(4 * n) + k), device_id_type=MESH,
         )
 
     def weights_there(n):
         return pltpu.make_async_remote_copy(
-            src_ref=wrel.at[0, :, my_lanes], dst_ref=wrel.at[n, :, my_lanes],
+            src_ref=wrel.at[:, 0, :, my_lanes], dst_ref=wrel.at[:, n, :, my_lanes],
             send_sem=w1_send.at[n], recv_sem=w1_recv.at[n],
             device_id=(j, 2 * ahead(4 * n) + k), device_id_type=MESH,
         )
@@ -139,7 +141,7 @@
 
     def weights_across(o):
         return pltpu.make_async_remote_copy(
-            src_ref=wrel.at[pl.ds(1, 3), :, my_lanes], dst_ref=wrel.at[pl.ds(1, 3), :, my_lanes],
+            src_ref=wrel.at[:, pl.ds(1, 3), :, my_lanes], dst_ref=wrel.at[:, pl.ds(1, 3), :, my_lanes],
             send_sem=w2_send.at[o], recv_sem=w2_recv.at[o],
             device_id=(at_sp(o // 4, o % 4), t), device_id_type=MESH,
         )
@@ -186,22 +188,19 @@
     for load in loads[7:]:
         load.wait()
 
+    def behind(way):
+        return i if way == 0 else 3 - i
+
     def source(way, n):
-        if n < 3:
-            return lax.rem(z - (n + 1) + N_Z, N_Z) if way == 0 else ahead(n + 1)
-        e = n - 3
-        if e < 4:
-            return 4 * prv + 3 - e if way == 0 else 4 * nxt + e
-        return 4 * opp + 3 - (e - 4) if way == 0 else 4 * opp + e - 4
-
-    def here(way, n):
-        return i >= n + 1 if way == 0 else i + n + 1 <= 3
-
-    def when_here(way, n, action):
-        if n < 3:
-            pl.when(here(way, n))(action)
-        else:
-            action()
+        e = n - behind(way)
+        if way == 0:
+            outside = jnp.where(e < 4, 4 * prv + 3 - e, 4 * opp + 7 - e)
+            return jnp.where(e < 0, lax.rem(z - (n + 1) + 2 * N_Z, N_Z), outside)
+        outside = jnp.where(e < 4, 4 * nxt + e, 4 * opp + e - 4)
+        return jnp.where(e < 0, lax.rem(z + n + 1, N_Z), outside)
+
+    def when_due(way, n, action):
+        pl.when((n >= 0) & (n < 6 + behind(way)))(action)
 
     def onward(way, n):
         src = source(way, n)
@@ -225,24 +224,22 @@
 
             to_core(src, way, n).start()
 
-        when_here(way, n, action)
+        when_due(way, n, action)
 
     def feats_of(src_z):
         return pl.ds(pl.multiple_of(src_z * 2 * FEATS, 2 * FEATS), 2 * FEATS)
 
     def compute(src_z, first=False):
-        feats = feats_of(src_z)
-        w = (wv_ref[feats, :].astype(jnp.float32).T * gain_ref[:, feats]).astype(jnp.bfloat16)
-        block = xt[feats, :]
-        term = jnp.dot(w, block, preferred_element_type=jnp.float32)
-        wide = block.astype(jnp.float32)
+        wide = xt[feats_of(src_z), :].astype(jnp.float32)
         sq = jnp.sum((wide * wide).reshape(2 * FEATS // 8, 8, ROWS), axis=0)
         if first:
-            acc[...] = term
             squares[...] = sq
         else:
-            acc[...] += term
             squares[...] += sq
+
+    def prepare(n):
+        feats = pl.ds(256 * n, 256)
+        wvt[:, feats] = (wv_ref[feats, :].astype(jnp.float32).T * gain_ref[:, feats]).astype(jnp.bfloat16)
 
     def process(way, n):
         def action():
@@ -250,23 +247,25 @@
             to_core(src, way, n).wait_recv()
             compute(src)
 
-        when_here(way, n, action)
-
-    for n in range(STEPS):
+        when_due(way, n, action)
+
+    for n in range(BEATS):
         for way in range(2):
-            take(way, n)
+            take(way, n - behind(way))
         if n == 0:
             to_core(z, 0, STEPS).wait_recv()
             compute(z, True)
         else:
             for way in range(2):
-                process(way, n - 1)
-        if n in (1, 2, 3):
-            phase = n - 1
+                process(way, n - 1 - behind(way))
+        if n < MODEL // 256:
+            prepare(n)
+        if n in (2, 3, 4):
+            phase = n - 2
             pl.semaphore_wait(near_sem.at[phase], 2)
             if phase < 2:
                 pass_on(phase + 1, across)
-        if n == 4:
+        if n == WEIGHT_BEAT:
             for m in range(1, 4):
                 weights_there(m).wait_recv()
             for o in SP_ORDER:
@@ -283,16 +282,13 @@
     for o in SP_ORDER:
         weights_across(o).wait_recv()
     for way in range(2):
-        process(way, STEPS - 1)
+        process(way, BEATS - 1 - behind(way))
 
     inverse = lax.rsqrt(jnp.sum(squares[...], axis=0, keepdims=True) * (1.0 / MODEL) + EPS)
-    both = jnp.dot(wrel[...].reshape(4 * 2 * CH, MODEL), xt[...], preferred_element_type=jnp.float32)
-    both = (both * inverse).astype(jnp.bfloat16).astype(jnp.float32)
+    gate = jnp.dot(wrel[1].reshape(NCH, MODEL), xt[...], preferred_element_type=jnp.float32)
+    gate = (gate * inverse).astype(jnp.bfloat16).astype(jnp.float32)
     for m in range(4):
-        b = lax.rem(quarter + m, 4)
-        key_scr[b] = both[2 * CH * m : 2 * CH * m + CH]
-        gate_scr[b] = both[2 * CH * m + CH : 2 * CH * m + 2 * CH]
-    key = key_scr[...].reshape(NCH, ROWS)
+        gate_scr[lax.rem(quarter + m, 4)] = gate[CH * m : CH * m + CH]
     u = gate_scr[...].reshape(NCH, ROWS) + bias + drift_ref[:, group_of(quarter)]
     log_decay = (jnp.minimum(u, 0.0) - jnp.log1p(jnp.exp(-jnp.abs(u)))) * (1.0 / GATE_NORM)
     blocks = ROWS // 128
@@ -322,10 +318,16 @@
     for o in ALL_ORDER:
         decays(o).start()
     d_got[4 * j + quarter] = d_msg[...]
+    key = jnp.dot(wrel[0].reshape(NCH, MODEL), xt[...], preferred_element_type=jnp.float32)
+    key = (key * inverse).astype(jnp.bfloat16).astype(jnp.float32)
+    for m in range(4):
+        key_scr[lax.rem(quarter + m, 4)] = key[CH * m : CH * m + CH]
+    key = key_scr[...].reshape(NCH, ROWS)
     weighted = jnp.concatenate(
         [(key[:, 128 * b : 128 * b + 128] * jnp.exp(rests[b])).astype(jnp.bfloat16) for b in range(blocks)], axis=1
     )
-    value = (acc[...] * inverse).astype(jnp.bfloat16)
+    value = jnp.dot(wvt[...], xt[...], preferred_element_type=jnp.float32)
+    value = (value * inverse).astype(jnp.bfloat16)
     partial = lax.dot_general(value, weighted, (((1,), (1,)), ((), ())), preferred_element_type=jnp.float32)
     msg[...] = partial.reshape(N_SP, VT, NCH)
 
@@ -349,7 +351,7 @@
 
                 to_core(source(way, n), way, n).wait_send()
 
-            when_here(way, n, action)
+            when_due(way, n, action)
     to_core(z, 0, STEPS).wait_send()
 
     @pl.when(i < 3)
@@ -477,8 +479,8 @@
             pltpu.VMEM((1, SPAN), f32),
             pltpu.VMEM((1, CH), bf16),
             pltpu.VMEM((HEADS, VT), f32),
-            pltpu.VMEM((4, 2 * CH, MODEL), bf16),
-            pltpu.VMEM((VALS, ROWS), f32),
+            pltpu.VMEM((2, 4, CH, MODEL), bf16),
+            pltpu.VMEM((VALS, MODEL), bf16),
             pltpu.VMEM((8, ROWS), f32),
             pltpu.VMEM((2, 128), f32),
             pltpu.VMEM((4, 2, 128), f32),

time: 186 us -> 78 us (0.42)
  Pallas kernels: 186 us -> 77.2 us
    pallas_call x1, Pallas kernels: 184 us -> 75.8 us  [body(): pl.pallas_call(kernel, out_shape=jax.ShapeDtypeStruct((CH + 8, 128), f32)...]
where the time goes in v5:
time: 78 us; the launch traced here: 77.8 us
  Pallas kernels  77.2 us (99%)
    pallas_call x1, Pallas kernels, body(): pl.pallas_call(kernel, out_shape=jax.ShapeDtypeStruct((CH + 8, 128), f32)...  75.8 us

profile of v5, /device:TPU:1, one launch (start us, length us, event | category | flops | bytes accessed | tf_op | source)
XLA Modules:
  0.0 77.8 jit_solution(16138142978694079646)
XLA Ops:
  0.6 75.8 %shard_map.104.packed_ref = f32[40,128]{1,0:T(8,128)} custom-call(bf16[64,2048]{1,0:T(8,128)(2,1)} %bitcast.7, f32[1,2048]{1,0:T(1,128)} %bitcast.10, bf16[32,2048]{1,0:T(8,128)(2,1)} %bitcast.8, bf16[32,2048]{1,0:T(8,128)(2,1)} %bitcast.9, bf16[2048,512]{1,0:T(8,128)(2,1)} %wv_hbm.1, f32[1,32]{1,0:T(1,128)} %bitcast.12, f32[1,2048]{1,0:T(1,128)} %bitcast.11, ...), custom_call_target="tpu_custom_call" | custom-call | tf_op jit(solution)/shard_map/pallas_call | solution.py:466
  76.4 1.4 %shard_map.105 = (bf16[32,32]{1,0:T(8,128)(2,1)}, f32[4,32]{1,0:T(4,128)}) custom-call(f32[40,128]{1,0:T(8,128)} %shard_map.104.packed_ref), custom_call_target="tpu_custom_call" | custom-call | tf_op jit(solution)/shard_map/pallas_call | solution.py:511

commit v6 on v5

--- a/solution.py
+++ b/solution.py
@@ -18,7 +18,9 @@
 HEADS = 4
 MODEL = N_TP * FEATS
 STEPS = 9
-BEATS = 12
+LAG = 2
+DEFER = 2
+BEATS = 9 + 3 * LAG
 WEIGHT_BEAT = 4
 HIGH = lax.Precision.HIGHEST
 
@@ -251,13 +253,13 @@
 
     for n in range(BEATS):
         for way in range(2):
-            take(way, n - behind(way))
+            take(way, n - LAG * behind(way))
         if n == 0:
             to_core(z, 0, STEPS).wait_recv()
             compute(z, True)
-        else:
+        if n >= DEFER:
             for way in range(2):
-                process(way, n - 1 - behind(way))
+                process(way, n - DEFER - LAG * behind(way))
         if n < MODEL // 256:
             prepare(n)
         if n in (2, 3, 4):
@@ -281,8 +283,9 @@
     summing = jnp.where((row_at > col_at) | (col_at >= 128), 1.0, 0.0).astype(jnp.bfloat16)
     for o in SP_ORDER:
         weights_across(o).wait_recv()
-    for way in range(2):
-        process(way, BEATS - 1 - behind(way))
+    for n in range(BEATS - DEFER, BEATS):
+        for way in range(2):
+            process(way, n - LAG * behind(way))
 
     inverse = lax.rsqrt(jnp.sum(squares[...], axis=0, keepdims=True) * (1.0 / MODEL) + EPS)
     gate = jnp.dot(wrel[1].reshape(NCH, MODEL), xt[...], preferred_element_type=jnp.float32)

time: 78 us -> 75.7 us (0.971)
  Pallas kernels: 77.2 us -> 74.9 us
    pallas_call x1, Pallas kernels: 75.8 us -> 73.5 us  [body(): pl.pallas_call(kernel, out_shape=jax.ShapeDtypeStruct((CH + 8, 128), f32)...]
where the time goes in v6:
time: 75.7 us; the launch traced here: 75.5 us
  Pallas kernels  74.9 us (99%)
    pallas_call x1, Pallas kernels, body(): pl.pallas_call(kernel, out_shape=jax.ShapeDtypeStruct((CH + 8, 128), f32)...  73.5 us

profile of v6, /device:TPU:1, one launch (start us, length us, event | category | flops | bytes accessed | tf_op | source)
XLA Modules:
  0.0 75.5 jit_solution(11385916929904476460)
XLA Ops:
  0.6 73.5 %shard_map.104.packed_ref = f32[40,128]{1,0:T(8,128)} custom-call(bf16[64,2048]{1,0:T(8,128)(2,1)} %bitcast.7, f32[1,2048]{1,0:T(1,128)} %bitcast.10, bf16[32,2048]{1,0:T(8,128)(2,1)} %bitcast.8, bf16[32,2048]{1,0:T(8,128)(2,1)} %bitcast.9, bf16[2048,512]{1,0:T(8,128)(2,1)} %wv_hbm.1, f32[1,32]{1,0:T(1,128)} %bitcast.12, f32[1,2048]{1,0:T(1,128)} %bitcast.11, ...), custom_call_target="tpu_custom_call" | custom-call | tf_op jit(solution)/shard_map/pallas_call | solution.py:469
  74.2 1.4 %shard_map.105 = (bf16[32,32]{1,0:T(8,128)(2,1)}, f32[4,32]{1,0:T(4,128)}) custom-call(f32[40,128]{1,0:T(8,128)} %shard_map.104.packed_ref), custom_call_target="tpu_custom_call" | custom-call | tf_op jit(solution)/shard_map/pallas_call | solution.py:514

commit v7 on v6

--- a/solution.py
+++ b/solution.py
@@ -21,7 +21,7 @@
 LAG = 2
 DEFER = 2
 BEATS = 9 + 3 * LAG
-WEIGHT_BEAT = 4
+WEIGHT_BEAT = 3
 HIGH = lax.Precision.HIGHEST
 
 
@@ -262,8 +262,8 @@
                 process(way, n - DEFER - LAG * behind(way))
         if n < MODEL // 256:
             prepare(n)
-        if n in (2, 3, 4):
-            phase = n - 2
+        if n in (0, 1, 2):
+            phase = n
             pl.semaphore_wait(near_sem.at[phase], 2)
             if phase < 2:
                 pass_on(phase + 1, across)
@@ -332,7 +332,7 @@
     value = jnp.dot(wvt[...], xt[...], preferred_element_type=jnp.float32)
     value = (value * inverse).astype(jnp.bfloat16)
     partial = lax.dot_general(value, weighted, (((1,), (1,)), ((), ())), preferred_element_type=jnp.float32)
-    msg[...] = partial.reshape(N_SP, VT, NCH)
+    msg[...] = partial.astype(jnp.bfloat16).reshape(N_SP, VT, NCH)
 
     def exchange(o):
         to = at_sp(o // 4, o % 4)
@@ -385,7 +385,7 @@
             piece = d_got[4 * n + g]
             mine = mine + jnp.where(g > quarter, piece, 0.0)
             later = later + piece
-        state = state + jnp.exp(mine) * got[n]
+        state = state + jnp.exp(mine) * got[n].astype(jnp.float32)
     lane_head = lax.broadcasted_iota(jnp.int32, (8, 128), 1) // VT
     pick_head = jnp.where(lane_head == lax.broadcasted_iota(jnp.int32, (8, 128), 0), 1.0, 0.0)
     head_rows = lax.dot_general(
@@ -489,8 +489,8 @@
             pltpu.VMEM((4, 2, 128), f32),
             pltpu.VMEM((4, CH, ROWS), f32),
             pltpu.VMEM((4, CH, ROWS), f32),
-            pltpu.VMEM((N_SP, VT, NCH), f32),
-            pltpu.VMEM((N_SP, VT, NCH), f32),
+            pltpu.VMEM((N_SP, VT, NCH), bf16),
+            pltpu.VMEM((N_SP, VT, NCH), bf16),
             pltpu.VMEM((1, 128), f32),
             pltpu.VMEM((4 * N_SP, 1, 128), f32),
             pltpu.VMEM((1, 128), f32),

time: 75.7 us -> 75.7 us (level)
  no operation moved by 1% of the time
where the time goes in v7:
time: 75.7 us; the launch traced here: 75.5 us
  Pallas kernels  74.9 us (99%)
    pallas_call x1, Pallas kernels, body(): pl.pallas_call(kernel, out_shape=jax.ShapeDtypeStruct((CH + 8, 128), f32)...  73.5 us

profile of v7, /device:TPU:1, one launch (start us, length us, event | category | flops | bytes accessed | tf_op | source)
XLA Modules:
  0.0 75.5 jit_solution(2329135096794306705)
XLA Ops:
  0.6 73.5 %shard_map.104.packed_ref = f32[40,128]{1,0:T(8,128)} custom-call(bf16[64,2048]{1,0:T(8,128)(2,1)} %bitcast.7, f32[1,2048]{1,0:T(1,128)} %bitcast.10, bf16[32,2048]{1,0:T(8,128)(2,1)} %bitcast.8, bf16[32,2048]{1,0:T(8,128)(2,1)} %bitcast.9, bf16[2048,512]{1,0:T(8,128)(2,1)} %wv_hbm.1, f32[1,32]{1,0:T(1,128)} %bitcast.12, f32[1,2048]{1,0:T(1,128)} %bitcast.11, ...), custom_call_target="tpu_custom_call" | custom-call | tf_op jit(solution)/shard_map/pallas_call | solution.py:469
  74.1 1.4 %shard_map.105 = (bf16[32,32]{1,0:T(8,128)(2,1)}, f32[4,32]{1,0:T(4,128)}) custom-call(f32[40,128]{1,0:T(8,128)} %shard_map.104.packed_ref), custom_call_target="tpu_custom_call" | custom-call | tf_op jit(solution)/shard_map/pallas_call | solution.py:514
